TPU v7x, 512 devices: a whole 4x4x16 slice. The times are simulated.
512 devices in a mesh: sp: 64 (over z, y), tp: 8 (over x, core).
Axes of the slice: x: 4, y: 4, z: 16, core: 2. Of those that a mesh axis runs over, the one named last changes fastest.
Arguments:
- normed: bfloat16 [16384, 2048], P(('sp', 'tp')), may hold values from -40 to 40
- query_weight: bfloat16 [2048, 2048], P(None, 'tp'), may hold values from -1.5 to 1.5
- key_weight: bfloat16 [2048, 2048], P(None, 'tp'), may hold values from -1 to 1
- value_weight: bfloat16 [2048, 2048], P(None, 'tp'), may hold values from -0.125 to 0.125
- pool_in_weight: bfloat16 [2048, 1024], P(None, 'tp'), may hold values from -0.125 to 0.125
- pool_weight: bfloat16 [8, 128, 128], P('tp'), may hold values from -0.5 to 0.5
- map_balance: float32 [8], replicated, may hold values from 0.3 to 0.8
- head_gain: float32 [256], replicated, may hold values from 0.1 to 1.9
- contrast_out_weight: bfloat16 [2048, 2048], P('tp'), may hold values from -0.109375 to 0.109375
- pool_out_weight: bfloat16 [1024, 2048], P('tp'), may hold values from -0.109375 to 0.109375
Outputs:
- layer_out: bfloat16 [16384, 2048], P(('sp', 'tp'))
All inputs are finite; a program needn't handle non-finite values.
Results may differ from a plain program's by a relative error of at most 0.03.
Values may be sent and summed in bfloat16 or wider, within the bound.
A program may use at most 128 MiB of HBM per device.

v0:
```python
import math

import jax
import jax.numpy as jnp
from jax import lax
from jax.sharding import PartitionSpec as P

reach_back = 15
norm_epsilon = 1e-06


def from_everyone(array, axis):
    copies = jnp.broadcast_to(array, (lax.axis_size(axis), *array.shape))
    return lax.all_to_all(copies, axis, split_axis=0, concat_axis=0, tiled=True)


def in_order(blocks, dim):
    lengths = list(blocks.shape[1:])
    lengths[dim] *= blocks.shape[0]
    return jnp.moveaxis(blocks, 0, dim).reshape(lengths)


def gathered_copies(array, axis, dim):
    blocks = from_everyone(array, axis)
    return in_order(blocks, dim)


def passed_along(block, axis, distance):
    devices = range(lax.axis_size(axis))
    route = [(i - distance, i) for i in devices if i - distance in devices]
    return lax.ppermute(block, axis, route)


def from_partner(block, axis, stride):
    count = lax.axis_size(axis)
    route = []
    for low in range(count):
        high = low | 1 << stride
        if high != low and high < count:
            route += [(low, high), (high, low)]
    return lax.ppermute(block, axis, route)


def shifted(array, axis, by):
    size = lax.axis_size(axis)
    return lax.ppermute(array, axis, [(i, (i + by) % size) for i in range(size)])


def as_sent(array):

    def short(part):
        return part.astype(jnp.bfloat16) if part.dtype == jnp.float32 else part

    return jax.tree.map(short, array)


def cut_along(array, dim, size):
    before, after = (array.shape[:dim], array.shape[dim + 1 :])
    return jnp.moveaxis(array.reshape(*before, size, -1, *after), dim, 0)


def summed_on_arrival(array, axis, dim):
    blocks = cut_along(array, dim, lax.axis_size(axis))
    arrived = lax.all_to_all(blocks, axis, split_axis=0, concat_axis=0, tiled=True)
    return arrived.astype(jnp.float32).sum(axis=0)


def attend(running, queries, key_rows, value_rows, query_first, key_first, score_scale):
    key_count = key_rows.shape[0]
    key_block = math.gcd(key_count, 1024)
    unit_count = queries.shape[1]
    heads_here = value_rows.shape[1]
    per_head = unit_count // heads_here
    query_count = queries.shape[0]
    query_order = query_first + lax.iota(jnp.int32, query_count)

    def key_step(block_index, carried):
        block_start = block_index * key_block

        def block_work(current):
            row_peak, row_total, weighted = current
            scores = (
                jnp.einsum("qud,kud->uqk", queries, key_rows, preferred_element_type=jnp.float32)
                * score_scale
            )
            key_order = key_first + block_start + lax.iota(jnp.int32, key_block)
            scores = jnp.where(
                key_order[None, None, :] <= query_order[None, :, None], scores, -jnp.inf
            )
            new_peak = jnp.maximum(row_peak, jnp.max(scores, axis=2))
            shrink = jnp.exp(row_peak - new_peak)
            raised = jnp.exp(scores - new_peak[:, :, None])
            row_total = row_total * shrink + jnp.sum(raised, axis=2)
            map_weights = raised.astype(jnp.bfloat16).reshape(
                heads_here, per_head, query_count, key_block
            )
            update = jnp.einsum(
                "hmqk,khe->hmqe", map_weights, value_rows, preferred_element_type=jnp.float32
            )
            weighted = weighted * shrink[:, :, None] + update.reshape(unit_count, query_count, -1)
            return (new_peak, row_total, weighted)

        def keep_state(current):
            return current

        return lax.cond(
            key_first + block_start <= query_first + query_count - 1,
            block_work,
            keep_state,
            carried,
        )

    return lax.fori_loop(0, key_count // key_block, key_step, running)


def fresh_state(unit_count, row_count, value_width):
    return (
        jnp.full((unit_count, row_count), -1e30, jnp.float32),
        jnp.zeros((unit_count, row_count), jnp.float32),
        jnp.zeros((unit_count, row_count, value_width), jnp.float32),
    )


def finished(running):
    row_peak, row_total, weighted = running
    return (weighted / row_total[:, :, None]).astype(jnp.bfloat16)


def joined_state(first, second):
    first_peak, first_total, first_weighted = first
    second_peak, second_total, second_weighted = second
    new_peak = jnp.maximum(first_peak, second_peak)
    first_shrink = jnp.exp(first_peak - new_peak)
    second_shrink = jnp.exp(second_peak - new_peak)
    new_total = first_total * first_shrink + second_total * second_shrink
    new_weighted = (
        first_weighted * first_shrink[:, :, None] + second_weighted * second_shrink[:, :, None]
    )
    return (new_peak, new_total, new_weighted)


def per_device(
    normed,
    query_weight,
    key_weight,
    value_weight,
    pool_in_weight,
    pool_weight,
    map_balance,
    head_gain,
    contrast_out_weight,
    pool_out_weight,
):
    tp_index = lax.axis_index("tp")
    sp_count = lax.axis_size("sp")
    sp_index = lax.axis_index("sp")
    head_dim = head_gain.shape[0] // 2
    value_width = 2 * head_dim
    query_cols = query_weight.shape[1]
    value_cols = value_weight.shape[1]
    unit_count = query_cols // head_dim
    heads_here = unit_count // 2
    project_incoming = gathered_copies(normed, "tp", 0)
    products = [
        jnp.dot(project_incoming, weight_part, preferred_element_type=jnp.float32)
        for weight_part in (query_weight, key_weight, value_weight, pool_in_weight)
    ]
    joined = jnp.concatenate(products, axis=1).astype(jnp.bfloat16)
    row_count = joined.shape[0]
    queries = joined[:, :query_cols].reshape(row_count, unit_count, head_dim)
    key_rows = joined[:, query_cols : 2 * query_cols].reshape(row_count, unit_count, head_dim)
    value_rows = joined[:, 2 * query_cols : 2 * query_cols + value_cols].reshape(
        row_count, heads_here, value_width
    )
    pool_input = joined[:, 2 * query_cols + value_cols :]
    pool_cols = pool_input.shape[1]
    upper_rim = passed_along(pool_input[row_count - reach_back :], "sp", 1)
    extended = jnp.concatenate([upper_rim, pool_input], axis=0).astype(jnp.float32)
    groups_here = pool_weight.shape[0]
    group_width = pool_weight.shape[1]
    group_index = tp_index * groups_here + lax.iota(jnp.int32, pool_cols) // group_width
    widths = jnp.left_shift(jnp.int32(2), group_index % 4)
    window_sum = jnp.zeros((row_count, pool_cols), jnp.float32)
    for offset in range(reach_back + 1):
        window_sum = window_sum + extended[
            reach_back - offset : reach_back - offset + row_count
        ] * (offset < widths)[None, :].astype(jnp.float32)
    position = sp_index * row_count + lax.iota(jnp.int32, row_count)
    counts = jnp.minimum(position[:, None] + 1, widths[None, :]).astype(jnp.float32)
    spread = (window_sum / counts - extended[reach_back:]).astype(jnp.bfloat16)
    mixed_groups = jnp.einsum(
        "tgc,gce->tge",
        spread.reshape(row_count, groups_here, group_width),
        pool_weight,
        preferred_element_type=jnp.float32,
    )
    pool_out = mixed_groups.reshape(row_count, pool_cols).astype(jnp.bfloat16)
    score_scale = head_dim ** (-0.5)
    level_count = sp_count.bit_length() - 1
    low_levels = level_count // 2
    band_size = 1 << low_levels
    band_count = sp_count // band_size
    member = sp_index % band_size
    band = sp_index // band_size
    band_queries = queries
    for bit in range(low_levels):
        received = from_partner(band_queries, "sp", bit)
        upper = member >> bit & 1 == 1
        band_queries = jnp.where(
            upper,
            jnp.concatenate([received, band_queries], axis=0),
            jnp.concatenate([band_queries, received], axis=0),
        )
    band_first = band * band_size * row_count
    running = fresh_state(unit_count, band_size * row_count, value_width)
    for step in range(band_count):
        if step == 0:
            key_piece, value_piece = (key_rows, value_rows)
        else:
            key_piece, value_piece = shifted((key_rows, value_rows), "sp", step * band_size)
        source = (sp_index - step * band_size) % sp_count
        running = attend(
            running,
            band_queries,
            key_piece,
            value_piece,
            band_first,
            source * row_count,
            score_scale,
        )
    for bit in range(low_levels - 1, -1, -1):
        half = running[0].shape[1] // 2
        upper = member >> bit & 1 == 1
        lower_part = jax.tree.map(lambda item: item[:, :half], running)
        upper_part = jax.tree.map(lambda item: item[:, half:], running)
        outgoing = jax.tree.map(
            lambda low, high: jnp.where(upper, low, high), lower_part, upper_part
        )
        kept = jax.tree.map(lambda low, high: jnp.where(upper, high, low), lower_part, upper_part)
        incoming = from_partner(
            (as_sent(outgoing[0]), as_sent(outgoing[1]), as_sent(outgoing[2])), "sp", bit
        )
        running = joined_state(kept, incoming)
    maps = finished(running)
    paired = maps.reshape(heads_here, 2, row_count, value_width)
    paired = lax.optimization_barrier(paired).astype(jnp.float32)
    head_first = tp_index * heads_here
    balance_here = lax.dynamic_slice_in_dim(map_balance, head_first, heads_here, 0)
    contrast = paired[:, 0] - balance_here[:, None, None] * paired[:, 1]
    mean_square = jnp.mean(contrast * contrast, axis=2, keepdims=True)
    contrast = contrast * lax.rsqrt(mean_square + norm_epsilon) * head_gain
    contrast_out = (
        contrast.astype(jnp.bfloat16)
        .transpose(1, 0, 2)
        .reshape(row_count, heads_here * value_width)
    )
    partial_value = jnp.dot(contrast_out, contrast_out_weight, preferred_element_type=jnp.float32)
    result = summed_on_arrival(
        (
            partial_value + jnp.dot(pool_out, pool_out_weight, preferred_element_type=jnp.float32)
        ).astype(jnp.bfloat16),
        "tp",
        0,
    )
    return result.astype(jnp.bfloat16)


def solution(mesh):
    return jax.shard_map(
        per_device,
        mesh=mesh,
        in_specs=(
            P(("sp", "tp"), None),
            P(None, "tp"),
            P(None, "tp"),
            P(None, "tp"),
            P(None, "tp"),
            P("tp", None, None),
            P(),
            P(),
            P("tp", None),
            P("tp", None),
        ),
        out_specs=P(("sp", "tp"), None),
        check_vma=False,
    )
```

profile of v0, /device:TPU:448, one launch (start us, length us, event | category | flops | bytes accessed | tf_op | source)
XLA Modules:
  0.0 306.2 jit_solution(13222507963534547856)
XLA Ops:
  6.6 15.8 %all-to-all-done = bf16[8,32,2048]{2,1,0:T(8,128)(2,1)S(1)} async-done(((bf16[8,32,2048]{2,1,0:T(8,128)(2,1)}), bf16[8,32,2048]{2,1,0:T(8,128)(2,1)S(1)}, u32[]{:S(2)}, u32[]{:S(2)}) %all-to-all-start) | async-done | bytes 1048608 | tf_op jit(solution)/shard_map/all_to_all | solution.py:14
  31.9 5.1 %collective-permute-start.1 = (bf16[512,2,128]{2,0,1:T(8,128)(2,1)}, bf16[512,2,128]{2,0,1:T(8,128)(2,1)}, u32[]{:S(2)}, u32[]{:S(2)}) collective-permute-start(bf16[512,2,128]{2,0,1:T(8,128)(2,1)} %maximum_select_fusion.2), channel_id=1, source_target_pairs={{0,16},{16,0},{8,24},{24,8},{32,48},{48,32},{40,56},{56,40},{64,80... | collective-permute-start | bytes 786440 | tf_op jit(solution)/shard_map/ppermute | solution.py:41
  51.1 5.2 %collective-permute-start.4 = (bf16[256,1,256]{2,0,1:T(8,128)(2,1)}, bf16[256,1,256]{2,0,1:T(8,128)(2,1)S(1)}, u32[]{:S(2)}, u32[]{:S(2)}) collective-permute-start(bf16[256,1,256]{2,0,1:T(8,128)(2,1)} %fusion.89), channel_id=1, source_target_pairs={{0,64},{8,72},{16,80},{24,88},{32,96},{40,104},{48,112},{56,120},{... | collective-permute-start | bytes 393224 | tf_op jit(solution)/shard_map/ppermute | solution.py:46
  56.2 6.4 %collective-permute-start.6 = (bf16[256,1,256]{2,0,1:T(8,128)(2,1)}, bf16[256,1,256]{2,0,1:T(8,128)(2,1)}, u32[]{:S(2)}, u32[]{:S(2)}) collective-permute-start(bf16[256,1,256]{2,0,1:T(8,128)(2,1)} %fusion.89), channel_id=1, source_target_pairs={{0,128},{8,136},{16,144},{24,152},{32,160},{40,168},{48,176},{56,1... | collective-permute-start | bytes 393224 | tf_op jit(solution)/shard_map/ppermute | solution.py:46
  66.4 34.9 %collective-permute-done.4 = bf16[256,1,256]{2,0,1:T(8,128)(2,1)S(1)} collective-permute-done((bf16[256,1,256]{2,0,1:T(8,128)(2,1)}, bf16[256,1,256]{2,0,1:T(8,128)(2,1)S(1)}, u32[]{:S(2)}, u32[]{:S(2)}) %collective-permute-start.4) | collective-permute-done | bytes 131104 | tf_op jit(solution)/shard_map/ppermute | solution.py:46
  104.6 11.5 %collective-permute-start.9 = (bf16[256,2,128]{2,0,1:T(8,128)(2,1)}, bf16[256,2,128]{2,0,1:T(8,128)(2,1)}, u32[]{:S(2)}, u32[]{:S(2)}) collective-permute-start(bf16[256,2,128]{2,0,1:T(8,128)(2,1)} %copy.23), channel_id=1, source_target_pairs={{0,256},{8,264},{16,272},{24,280},{32,288},{40,296},{48,304},{56,3... | collective-permute-start | bytes 393224 | tf_op jit(solution)/shard_map/ppermute | solution.py:46
  119.3 8.3 %collective-permute-start.11 = (bf16[256,2,128]{2,0,1:T(8,128)(2,1)}, bf16[256,2,128]{2,0,1:T(8,128)(2,1)}, u32[]{:S(2)}, u32[]{:S(2)}) collective-permute-start(bf16[256,2,128]{2,0,1:T(8,128)(2,1)} %copy.23), channel_id=1, source_target_pairs={{0,320},{8,328},{16,336},{24,344},{32,352},{40,360},{48,368},{56,3... | collective-permute-start | bytes 393224 | tf_op jit(solution)/shard_map/ppermute | solution.py:46
  130.7 7.0 %collective-permute-start.12 = (bf16[256,1,256]{2,0,1:T(8,128)(2,1)}, bf16[256,1,256]{2,0,1:T(8,128)(2,1)}, u32[]{:S(2)}, u32[]{:S(2)}) collective-permute-start(bf16[256,1,256]{2,0,1:T(8,128)(2,1)} %fusion.89), channel_id=1, source_target_pairs={{0,320},{8,328},{16,336},{24,344},{32,352},{40,360},{48,368},{56,3... | collective-permute-start | bytes 393224 | tf_op jit(solution)/shard_map/ppermute | solution.py:46
  138.9 5.7 %collective-permute-start.13 = (bf16[256,2,128]{2,0,1:T(8,128)(2,1)}, bf16[256,2,128]{2,0,1:T(8,128)(2,1)}, u32[]{:S(2)}, u32[]{:S(2)}) collective-permute-start(bf16[256,2,128]{2,0,1:T(8,128)(2,1)} %copy.23), channel_id=1, source_target_pairs={{0,384},{8,392},{16,400},{24,408},{32,416},{40,424},{48,432},{56,4... | collective-permute-start | bytes 393224 | tf_op jit(solution)/shard_map/ppermute | solution.py:46
  153.3 7.9 %collective-permute-start.16 = (bf16[256,1,256]{2,0,1:T(8,128)(2,1)}, bf16[256,1,256]{2,0,1:T(8,128)(2,1)}, u32[]{:S(2)}, u32[]{:S(2)}) collective-permute-start(bf16[256,1,256]{2,0,1:T(8,128)(2,1)} %fusion.89), channel_id=1, source_target_pairs={{0,448},{8,456},{16,464},{24,472},{32,480},{40,488},{48,496},{56,5... | collective-permute-start | bytes 393224 | tf_op jit(solution)/shard_map/ppermute | solution.py:46
  163.0 7.1 %conditional.8 = ((f32[2,2048]{1,0:T(2,128)S(1)}, f32[2,2048]{1,0:T(2,128)S(1)}, f32[2,2048,256]{2,1,0:T(8,128)})) conditional(s32[]{:T(128)} %convert_element_type.280, (f32[2,2048]{1,0:T(2,128)S(1)}, f32[2,2048]{1,0:T(2,128)S(1)}, f32[2,2048,256]{2,1,0:T(8,128)}) %tuple.96, (s32[]{:T(128)}, s32[2048]{0:T(1024)S(1)}, ...), branch_computations={%region_0.1_spmd, %region_1.4_spmd} | conditional | flops 819470592 | bytes 24651812 | solution.py:106
  170.2 8.0 %conditional.9 = ((f32[2,2048]{1,0:T(2,128)S(1)}, f32[2,2048]{1,0:T(2,128)S(1)}, f32[2,2048,256]{2,1,0:T(8,128)})) conditional(s32[]{:T(128)} %convert_element_type.279, (f32[2,2048]{1,0:T(2,128)S(1)}, f32[2,2048]{1,0:T(2,128)S(1)}, f32[2,2048,256]{2,1,0:T(8,128)}) %get-tuple-element.787, (s32[]{:T(128)}, s32[2048]{0:T(1024)S(1)}, ...), branch_computations={%region_4.5_spmd, %region_5.8_spmd} | conditional | flops 819470592 | bytes 25176128 | solution.py:106
  178.2 8.0 %conditional.10 = ((f32[2,2048]{1,0:T(2,128)S(1)}, f32[2,2048]{1,0:T(2,128)S(1)}, f32[2,2048,256]{2,1,0:T(8,128)})) conditional(s32[]{:T(128)} %convert_element_type.278, (f32[2,2048]{1,0:T(2,128)S(1)}, f32[2,2048]{1,0:T(2,128)S(1)}, f32[2,2048,256]{2,1,0:T(8,128)}) %get-tuple-element.788, (s32[]{:T(128)}, s32[2048]{0:T(1024)S(1)}, ...), branch_computations={%region_8.9_spmd, %region_9.12_spmd} | conditional | flops 819470592 | bytes 24651812 | solution.py:106
  186.2 8.0 %conditional.11 = ((f32[2,2048]{1,0:T(2,128)S(1)}, f32[2,2048]{1,0:T(2,128)S(1)}, f32[2,2048,256]{2,1,0:T(8,128)})) conditional(s32[]{:T(128)} %convert_element_type.277, (f32[2,2048]{1,0:T(2,128)S(1)}, f32[2,2048]{1,0:T(2,128)S(1)}, f32[2,2048,256]{2,1,0:T(8,128)}) %get-tuple-element.789, (s32[]{:T(128)}, s32[2048]{0:T(1024)S(1)}, ...), branch_computations={%region_12.13_spmd, %region_13.16_spmd} | conditional | flops 819470592 | bytes 24651812 | solution.py:106
  194.1 8.0 %conditional.12 = ((f32[2,2048]{1,0:T(2,128)S(1)}, f32[2,2048]{1,0:T(2,128)S(1)}, f32[2,2048,256]{2,1,0:T(8,128)})) conditional(s32[]{:T(128)} %convert_element_type.276, (f32[2,2048]{1,0:T(2,128)S(1)}, f32[2,2048]{1,0:T(2,128)S(1)}, f32[2,2048,256]{2,1,0:T(8,128)}) %get-tuple-element.790, (s32[]{:T(128)}, s32[2048]{0:T(1024)S(1)}, ...), branch_computations={%region_16.17_spmd, %region_17.20_spmd} | conditional | flops 819470592 | bytes 24651812 | solution.py:106
  202.1 8.2 %conditional.13 = ((f32[2,2048]{1,0:T(2,128)S(1)}, f32[2,2048]{1,0:T(2,128)S(1)}, f32[2,2048,256]{2,1,0:T(8,128)})) conditional(s32[]{:T(128)} %convert_element_type.275, (f32[2,2048]{1,0:T(2,128)S(1)}, f32[2,2048]{1,0:T(2,128)S(1)}, f32[2,2048,256]{2,1,0:T(8,128)}) %get-tuple-element.791, (s32[]{:T(128)}, s32[2048]{0:T(1024)S(1)}, ...), branch_computations={%region_20.21_spmd, %region_21.24_spmd} | conditional | flops 819470592 | bytes 24651812 | solution.py:106
  205.6 4.6 %multiply_add_fusion.10 = f32[2,2048,256]{2,1,0:T(8,128)} fusion(f32[2,2048,256]{2,1,0:T(8,128)} %get-tuple-element.571, f32[2,2048,256]{1,2,0:T(8,128)S(1)} %get-tuple-element.718, f32[2,2048]{1,0:T(2,128)S(1)} %get-tuple-element.691, f32[2,2048]{1,0:T(2,128)S(1)} %max.29, pred[2048,256]{0,1:T(8,128)(4,1)S(1)} %broadcast_compare_fusion.5, ...), kind=kOutput, calls=%fused_computation.85 | convolution fusion | flops 543162368 | bytes 13271040 | tf_op jit(solution)/shard_map/while/body/eval_jaxpr/cond/branch_1_fun/hmqk,khe->hmqe/dot_general | solution.py:97
  210.3 8.0 %conditional.14 = ((f32[2,2048]{1,0:T(2,128)S(1)}, f32[2,2048]{1,0:T(2,128)S(1)}, f32[2,2048,256]{2,1,0:T(8,128)})) conditional(s32[]{:T(128)} %convert_element_type.274, (f32[2,2048]{1,0:T(2,128)S(1)}, f32[2,2048]{1,0:T(2,128)S(1)}, f32[2,2048,256]{2,1,0:T(8,128)}) %get-tuple-element.792, (s32[]{:T(128)}, s32[2048]{0:T(1024)S(1)}, ...), branch_computations={%region_24.25_spmd, %region_25.28_spmd} | conditional | flops 819470592 | bytes 24651812 | solution.py:106
  218.3 8.0 %conditional.15 = (f32[2,2048,256]{2,1,0:T(8,128)}, f32[2,2048]{1,0:T(2,128)S(1)}, f32[2,2048]{1,0:T(2,128)S(1)}) conditional(s32[]{:T(128)} %convert_element_type.273, (f32[2,2048]{1,0:T(2,128)S(1)}, f32[2,2048]{1,0:T(2,128)S(1)}, f32[2,2048,256]{2,1,0:T(8,128)}) %get-tuple-element.793, (s32[]{:T(128)}, s32[2048]{0:T(1024)S(1)}, ...), branch_computations={%region_28.29_spmd.clone, %region_29.32_spmd.clone} | conditional | flops 819470592 | bytes 24651804 | solution.py:106
  238.7 5.3 %collective-permute-start.24 = (bf16[2,512]{1,0:T(2,128)(2,1)S(1)}, bf16[2,512]{1,0:T(2,128)(2,1)S(1)}, u32[]{:S(2)}, u32[]{:S(2)}) collective-permute-start(bf16[2,512]{1,0:T(2,128)(2,1)S(1)} %select_convert_fusion.5), channel_id=1, source_target_pairs={{0,16},{16,0},{8,24},{24,8},{32,48},{48,32},{40,56},{56,40},{64,80... | collective-permute-start | bytes 6152 | tf_op jit(solution)/shard_map/ppermute | solution.py:41
  248.1 5.1 %collective-permute-done.18 = bf16[2,1024,256]{2,1,0:T(8,128)(2,1)S(1)} collective-permute-done((bf16[2,1024,256]{2,1,0:T(8,128)(2,1)S(1)}, bf16[2,1024,256]{2,1,0:T(8,128)(2,1)S(1)}, u32[]{:S(2)}, u32[]{:S(2)}) %collective-permute-start.18) | collective-permute-done | bytes 1048608 | tf_op jit(solution)/shard_map/ppermute | solution.py:41
  264.3 7.0 %collective-permute-done.20 = bf16[2,512,256]{2,1,0:T(8,128)(2,1)S(1)} collective-permute-done((bf16[2,512,256]{2,1,0:T(8,128)(2,1)S(1)}, bf16[2,512,256]{2,1,0:T(8,128)(2,1)S(1)}, u32[]{:S(2)}, u32[]{:S(2)}) %collective-permute-start.20) | collective-permute-done | bytes 524320 | tf_op jit(solution)/shard_map/ppermute | solution.py:41
  274.5 5.6 %collective-permute-done.22 = bf16[2,256,256]{2,1,0:T(8,128)(2,1)S(1)} collective-permute-done((bf16[2,256,256]{2,1,0:T(8,128)(2,1)S(1)}, bf16[2,256,256]{2,1,0:T(8,128)(2,1)S(1)}, u32[]{:S(2)}, u32[]{:S(2)}) %collective-permute-start.22) | collective-permute-done | bytes 262176 | tf_op jit(solution)/shard_map/ppermute | solution.py:41
  286.2 19.3 %all_to_all.10 = bf16[8,32,2048]{2,1,0:T(8,128)(2,1)S(1)} all-to-all(bf16[8,32,2048]{2,1,0:T(8,128)(2,1)S(1)} %bitcast.84), channel_id=1, replica_groups=mesh['sp'=64,'tp'=8] {'tp'}, dimensions={0} | all-to-all | bytes 2097152 | tf_op jit(solution)/shard_map/all_to_all | solution.py:64
  (175 shorter events, 150.1 us)
Async XLA Ops:
  2.2 20.2 %all-to-all-start = ((bf16[8,32,2048]{2,1,0:T(8,128)(2,1)}), bf16[8,32,2048]{2,1,0:T(8,128)(2,1)S(1)}, u32[]{:S(2)}, u32[]{:S(2)}) async-start(bf16[8,32,2048]{2,1,0:T(8,128)(2,1)} %broadcast_in_dim.148), calls=%async_computation | async-start | bytes 2097152 | tf_op jit(solution)/shard_map/all_to_all | solution.py:14
  31.9 11.6 %collective-permute-start.1 = (bf16[512,2,128]{2,0,1:T(8,128)(2,1)}, bf16[512,2,128]{2,0,1:T(8,128)(2,1)}, u32[]{:S(2)}, u32[]{:S(2)}) collective-permute-start(bf16[512,2,128]{2,0,1:T(8,128)(2,1)} %maximum_select_fusion.2), channel_id=1, source_target_pairs={{0,16},{16,0},{8,24},{24,8},{32,48},{48,32},{40,56},{56,40},{64,80... | collective-permute-start | bytes 786440 | tf_op jit(solution)/shard_map/ppermute | solution.py:41
  38.3 24.3 %collective-permute-start.3 = (bf16[256,2,128]{2,0,1:T(8,128)(2,1)}, bf16[256,2,128]{2,0,1:T(8,128)(2,1)}, u32[]{:S(2)}, u32[]{:S(2)}) collective-permute-start(bf16[256,2,128]{2,0,1:T(8,128)(2,1)} %copy.23), channel_id=1, source_target_pairs={{0,64},{8,72},{16,80},{24,88},{32,96},{40,104},{48,112},{56,120},{... | collective-permute-start | bytes 393224 | tf_op jit(solution)/shard_map/ppermute | solution.py:46
  40.2 64.4 %collective-permute-start.5 = (bf16[256,2,128]{2,0,1:T(8,128)(2,1)}, bf16[256,2,128]{2,0,1:T(8,128)(2,1)}, u32[]{:S(2)}, u32[]{:S(2)}) collective-permute-start(bf16[256,2,128]{2,0,1:T(8,128)(2,1)} %copy.23), channel_id=1, source_target_pairs={{0,128},{8,136},{16,144},{24,152},{32,160},{40,168},{48,176},{56,1... | collective-permute-start | bytes 393224 | tf_op jit(solution)/shard_map/ppermute | solution.py:46
  44.9 107.6 %collective-permute-start.2 = (bf16[1024,2,128]{2,0,1:T(8,128)(2,1)S(1)}, bf16[1024,2,128]{2,0,1:T(8,128)(2,1)S(1)}, u32[]{:S(2)}, u32[]{:S(2)}) collective-permute-start(bf16[1024,2,128]{2,0,1:T(8,128)(2,1)S(1)} %maximum_select_fusion.1), channel_id=1, source_target_pairs={{0,32},{32,0},{8,40},{40,8},{16,48},{48,16},{24,56},{56,24},{64,96... | collective-permute-start | bytes 1572872 | tf_op jit(solution)/shard_map/ppermute | solution.py:41
  51.1 50.3 %collective-permute-start.4 = (bf16[256,1,256]{2,0,1:T(8,128)(2,1)}, bf16[256,1,256]{2,0,1:T(8,128)(2,1)S(1)}, u32[]{:S(2)}, u32[]{:S(2)}) collective-permute-start(bf16[256,1,256]{2,0,1:T(8,128)(2,1)} %fusion.89), channel_id=1, source_target_pairs={{0,64},{8,72},{16,80},{24,88},{32,96},{40,104},{48,112},{56,120},{... | collective-permute-start | bytes 393224 | tf_op jit(solution)/shard_map/ppermute | solution.py:46
  56.2 60.0 %collective-permute-start.6 = (bf16[256,1,256]{2,0,1:T(8,128)(2,1)}, bf16[256,1,256]{2,0,1:T(8,128)(2,1)}, u32[]{:S(2)}, u32[]{:S(2)}) collective-permute-start(bf16[256,1,256]{2,0,1:T(8,128)(2,1)} %fusion.89), channel_id=1, source_target_pairs={{0,128},{8,136},{16,144},{24,152},{32,160},{40,168},{48,176},{56,1... | collective-permute-start | bytes 393224 | tf_op jit(solution)/shard_map/ppermute | solution.py:46
  62.6 56.6 %collective-permute-start.7 = (bf16[256,2,128]{2,0,1:T(8,128)(2,1)}, bf16[256,2,128]{2,0,1:T(8,128)(2,1)}, u32[]{:S(2)}, u32[]{:S(2)}) collective-permute-start(bf16[256,2,128]{2,0,1:T(8,128)(2,1)} %copy.23), channel_id=1, source_target_pairs={{0,192},{8,200},{16,208},{24,216},{32,224},{40,232},{48,240},{56,2... | collective-permute-start | bytes 393224 | tf_op jit(solution)/shard_map/ppermute | solution.py:46
  101.3 29.3 %collective-permute-start.8 = (bf16[256,1,256]{2,0,1:T(8,128)(2,1)}, bf16[256,1,256]{2,0,1:T(8,128)(2,1)}, u32[]{:S(2)}, u32[]{:S(2)}) collective-permute-start(bf16[256,1,256]{2,0,1:T(8,128)(2,1)} %fusion.89), channel_id=1, source_target_pairs={{0,192},{8,200},{16,208},{24,216},{32,224},{40,232},{48,240},{56,2... | collective-permute-start | bytes 393224 | tf_op jit(solution)/shard_map/ppermute | solution.py:46
  104.6 34.2 %collective-permute-start.9 = (bf16[256,2,128]{2,0,1:T(8,128)(2,1)}, bf16[256,2,128]{2,0,1:T(8,128)(2,1)}, u32[]{:S(2)}, u32[]{:S(2)}) collective-permute-start(bf16[256,2,128]{2,0,1:T(8,128)(2,1)} %copy.23), channel_id=1, source_target_pairs={{0,256},{8,264},{16,272},{24,280},{32,288},{40,296},{48,304},{56,3... | collective-permute-start | bytes 393224 | tf_op jit(solution)/shard_map/ppermute | solution.py:46
  116.2 31.0 %collective-permute-start.10 = (bf16[256,1,256]{2,0,1:T(8,128)(2,1)}, bf16[256,1,256]{2,0,1:T(8,128)(2,1)S(1)}, u32[]{:S(2)}, u32[]{:S(2)}) collective-permute-start(bf16[256,1,256]{2,0,1:T(8,128)(2,1)} %fusion.89), channel_id=1, source_target_pairs={{0,256},{8,264},{16,272},{24,280},{32,288},{40,296},{48,304},{56,3... | collective-permute-start | bytes 393224 | tf_op jit(solution)/shard_map/ppermute | solution.py:46
  119.3 30.4 %collective-permute-start.11 = (bf16[256,2,128]{2,0,1:T(8,128)(2,1)}, bf16[256,2,128]{2,0,1:T(8,128)(2,1)}, u32[]{:S(2)}, u32[]{:S(2)}) collective-permute-start(bf16[256,2,128]{2,0,1:T(8,128)(2,1)} %copy.23), channel_id=1, source_target_pairs={{0,320},{8,328},{16,336},{24,344},{32,352},{40,360},{48,368},{56,3... | collective-permute-start | bytes 393224 | tf_op jit(solution)/shard_map/ppermute | solution.py:46
  130.7 71.4 %collective-permute-start.12 = (bf16[256,1,256]{2,0,1:T(8,128)(2,1)}, bf16[256,1,256]{2,0,1:T(8,128)(2,1)}, u32[]{:S(2)}, u32[]{:S(2)}) collective-permute-start(bf16[256,1,256]{2,0,1:T(8,128)(2,1)} %fusion.89), channel_id=1, source_target_pairs={{0,320},{8,328},{16,336},{24,344},{32,352},{40,360},{48,368},{56,3... | collective-permute-start | bytes 393224 | tf_op jit(solution)/shard_map/ppermute | solution.py:46
  138.9 71.4 %collective-permute-start.13 = (bf16[256,2,128]{2,0,1:T(8,128)(2,1)}, bf16[256,2,128]{2,0,1:T(8,128)(2,1)}, u32[]{:S(2)}, u32[]{:S(2)}) collective-permute-start(bf16[256,2,128]{2,0,1:T(8,128)(2,1)} %copy.23), channel_id=1, source_target_pairs={{0,384},{8,392},{16,400},{24,408},{32,416},{40,424},{48,432},{56,4... | collective-permute-start | bytes 393224 | tf_op jit(solution)/shard_map/ppermute | solution.py:46
  147.2 63.1 %collective-permute-start.14 = (bf16[256,1,256]{2,0,1:T(8,128)(2,1)}, bf16[256,1,256]{2,0,1:T(8,128)(2,1)}, u32[]{:S(2)}, u32[]{:S(2)}) collective-permute-start(bf16[256,1,256]{2,0,1:T(8,128)(2,1)} %fusion.89), channel_id=1, source_target_pairs={{0,384},{8,392},{16,400},{24,408},{32,416},{40,424},{48,432},{56,4... | collective-permute-start | bytes 393224 | tf_op jit(solution)/shard_map/ppermute | solution.py:46
  149.7 68.7 %collective-permute-start.15 = (bf16[256,2,128]{2,0,1:T(8,128)(2,1)}, bf16[256,2,128]{2,0,1:T(8,128)(2,1)}, u32[]{:S(2)}, u32[]{:S(2)}) collective-permute-start(bf16[256,2,128]{2,0,1:T(8,128)(2,1)} %copy.23), channel_id=1, source_target_pairs={{0,448},{8,456},{16,464},{24,472},{32,480},{40,488},{48,496},{56,5... | collective-permute-start | bytes 393224 | tf_op jit(solution)/shard_map/ppermute | solution.py:46
  153.3 65.0 %collective-permute-start.16 = (bf16[256,1,256]{2,0,1:T(8,128)(2,1)}, bf16[256,1,256]{2,0,1:T(8,128)(2,1)}, u32[]{:S(2)}, u32[]{:S(2)}) collective-permute-start(bf16[256,1,256]{2,0,1:T(8,128)(2,1)} %fusion.89), channel_id=1, source_target_pairs={{0,448},{8,456},{16,464},{24,472},{32,480},{40,488},{48,496},{56,5... | collective-permute-start | bytes 393224 | tf_op jit(solution)/shard_map/ppermute | solution.py:46
  226.3 10.2 %collective-permute-start.17 = (bf16[2,1024]{1,0:T(2,128)(2,1)S(1)}, bf16[2,1024]{1,0:T(2,128)(2,1)S(1)}, u32[]{:S(2)}, u32[]{:S(2)}) collective-permute-start(bf16[2,1024]{1,0:T(2,128)(2,1)S(1)} %select_convert_fusion.4), channel_id=1, source_target_pairs={{0,32},{32,0},{8,40},{40,8},{16,48},{48,16},{24,56},{56,24},{64,96... | collective-permute-start | bytes 12296 | tf_op jit(solution)/shard_map/ppermute | solution.py:41
  234.6 18.6 %collective-permute-start.18 = (bf16[2,1024,256]{2,1,0:T(8,128)(2,1)S(1)}, bf16[2,1024,256]{2,1,0:T(8,128)(2,1)S(1)}, u32[]{:S(2)}, u32[]{:S(2)}) collective-permute-start(bf16[2,1024,256]{2,1,0:T(8,128)(2,1)S(1)} %select_convert_fusion), channel_id=1, source_target_pairs={{0,32},{32,0},{8,40},{40,8},{16,48},{48,16},{24,56},{56,24},{64,96... | collective-permute-start | bytes 3145736 | tf_op jit(solution)/shard_map/ppermute | solution.py:41
  236.6 11.5 %collective-permute-start.19 = (bf16[2,512]{1,0:T(2,128)(2,1)S(1)}, bf16[2,512]{1,0:T(2,128)(2,1)S(1)}, u32[]{:S(2)}, u32[]{:S(2)}) collective-permute-start(bf16[2,512]{1,0:T(2,128)(2,1)S(1)} %select_convert_fusion.6), channel_id=1, source_target_pairs={{0,16},{16,0},{8,24},{24,8},{32,48},{48,32},{40,56},{56,40},{64,80... | collective-permute-start | bytes 6152 | tf_op jit(solution)/shard_map/ppermute | solution.py:41
  245.5 29.0 %collective-permute-start.26 = (bf16[15,128]{1,0:T(8,128)(2,1)S(1)}, bf16[15,128]{1,0:T(8,128)(2,1)S(1)}, u32[]{:S(2)}, u32[]{:S(2)}) collective-permute-start(bf16[15,128]{1,0:T(8,128)(2,1)S(1)} %slice.271), channel_id=1, source_target_pairs={{0,8},{8,16},{16,24},{24,32},{32,40},{40,48},{48,56},{56,64},{64,7... | collective-permute-start | bytes 11528 | tf_op jit(solution)/shard_map/ppermute | solution.py:31
  255.9 15.4 %collective-permute-start.20 = (bf16[2,512,256]{2,1,0:T(8,128)(2,1)S(1)}, bf16[2,512,256]{2,1,0:T(8,128)(2,1)S(1)}, u32[]{:S(2)}, u32[]{:S(2)}) collective-permute-start(bf16[2,512,256]{2,1,0:T(8,128)(2,1)S(1)} %select_convert_fusion.1), channel_id=1, source_target_pairs={{0,16},{16,0},{8,24},{24,8},{32,48},{48,32},{40,56},{56,40},{64,80... | collective-permute-start | bytes 1572872 | tf_op jit(solution)/shard_map/ppermute | solution.py:41
  258.2 16.3 %collective-permute-start.21 = (bf16[2,256]{1,0:T(2,128)(2,1)S(1)}, bf16[2,256]{1,0:T(2,128)(2,1)S(1)}, u32[]{:S(2)}, u32[]{:S(2)}) collective-permute-start(bf16[2,256]{1,0:T(2,128)(2,1)S(1)} %select_convert_fusion.8), channel_id=1, source_target_pairs={{0,8},{8,0},{16,24},{24,16},{32,40},{40,32},{48,56},{56,48},{64,72... | collective-permute-start | bytes 3080 | tf_op jit(solution)/shard_map/ppermute | solution.py:41
  262.4 12.1 %collective-permute-start.25 = (bf16[2,256]{1,0:T(2,128)(2,1)S(1)}, bf16[2,256]{1,0:T(2,128)(2,1)S(1)}, u32[]{:S(2)}, u32[]{:S(2)}) collective-permute-start(bf16[2,256]{1,0:T(2,128)(2,1)S(1)} %select_convert_fusion.7), channel_id=1, source_target_pairs={{0,8},{8,0},{16,24},{24,16},{32,40},{40,32},{48,56},{56,48},{64,72... | collective-permute-start | bytes 3080 | tf_op jit(solution)/shard_map/ppermute | solution.py:41
  (14 other events, 632.5 us)
where the time goes:
time: 308 us; the launch traced here: 306 us
  starting transfers between devices  118 us (38%)
  waiting for transfers between devices  75.7 us (25%)
  matrix products  62.4 us (20%)
  other arithmetic  22.8 us (7%)
  blocking collectives  19.3 us (6%)
  local copies, waits for them, and re-layouts  6.81 us (2%)
    ppermute x14, starting transfers between devices, shifted(): lax.ppermute(array, axis, [(i, (i + by) % size) for i in range(size)])  72.4 us
    ppermute x14, waiting for transfers between devices, shifted(): lax.ppermute(array, axis, [(i, (i + by) % size) for i in range(size)])  38.8 us
    ppermute x12, starting transfers between devices, from_partner(): return lax.ppermute(block, axis, route)  38.5 us
    dot_general x8, matrix products, block_work(): jnp.einsum('hmqk,khe->hmqe', map_weights, value_rows, preferred_element_t...  37.1 us
    ppermute x12, waiting for transfers between devices, from_partner(): return lax.ppermute(block, axis, route)  21 us
    all_to_all x1, blocking collectives, summed_on_arrival(): lax.all_to_all(blocks, axis, split_axis=0, concat_axis=0, tiled=True)  19.3 us
    all_to_all x1, waiting for transfers between devices, from_everyone(): return lax.all_to_all(copies, axis, split_axis=0, concat_axis=0, tiled=True)  15.8 us
    dot_general x8, matrix products, block_work(): jnp.einsum('qud,kud->uqk', queries, key_rows, preferred_element_type=jnp....  14.3 us
  transfers between devices with their start and end apart: 28, of which 8 were waited for; matrix products, arithmetic and copies ran while one was open for 23% of the time, Pallas kernels for 0%

commit v1 on v0

v1 whole, which is shorter than its diff:
```python
import functools
import math

import jax
import jax.numpy as jnp
from jax import lax
from jax.experimental import pallas as pl
from jax.experimental.pallas import tpu as pltpu
from jax.sharding import PartitionSpec as P

MESH = pl.DeviceIdType.MESH
F32 = jnp.float32
BF16 = jnp.bfloat16
Y = 4
X = 4
NEG = -1e30
norm_epsilon = 1e-06


def kernel(
    zn,
    normed,
    wq_h,
    wk_h,
    wv_h,
    wp_h,
    pool_weight,
    balance,
    gain,
    cow_h,
    pow_h,
    out,
    xg,
    wq,
    wk,
    wv,
    wp,
    cow,
    pow_,
    q_all,
    k_all,
    v_all,
    acc,
    m_s,
    l_s,
    pin,
    rim,
    ext,
    pool_part,
    ps,
    pst,
    r2,
    r2t,
    rn,
    rnt,
    co,
    part,
    pr,
    xs,
    xr2,
    xrn,
    w_sem,
    xg_send,
    xg_recv,
    up_send,
    dn_send,
    kv_up_recv,
    kv_dn_recv,
    q_send,
    q_recv,
    h_sem,
    ps_send,
    ps_recv,
    pr_send,
    pr_recv,
    xs_send,
    xs_recv,
):
    sp = lax.axis_index("sp")
    tp = lax.axis_index("tp")
    nsp = zn * Y
    z, y = sp // Y, sp % Y
    x, core = tp // 2, tp % 2
    up_hops = zn // 2
    dn_hops = zn // 2 - 1

    def at(zz, yy, xx, cc):
        return {"sp": zz * Y + yy, "tp": xx * 2 + cc}

    partner = at(z, y, x, 1 - core)
    xr, xl = (x + 1) % X, (x + X - 1) % X
    x2 = (x + 2) % X
    yr, yl = (y + 1) % Y, (y + Y - 1) % Y
    y2 = (y + 2) % Y
    zu, zd = (z + 1) % zn, (z + zn - 1) % zn
    x_right, x_left = at(z, y, xr, core), at(z, y, xl, core)
    y_right, y_left = at(z, yr, x, core), at(z, yl, x, core)
    z_up, z_down = at(zu, y, x, core), at(zd, y, x, core)
    next_sp = {"sp": (sp + 1) % nsp, "tp": tp}
    prev_sp = {"sp": (sp + nsp - 1) % nsp, "tp": tp}

    weights = [
        pltpu.make_async_copy(src, dst, w_sem.at[i])
        for i, (src, dst) in enumerate(
            ((wk_h, wk), (wv_h, wv), (wq_h, wq), (wp_h, wp), (pow_h, pow_), (cow_h, cow))
        )
    ]
    for copy in weights:
        copy.start()

    barrier = pltpu.get_barrier_semaphore()
    peers = (partner, x_right, x_left, y_right, y_left, z_up, z_down, next_sp, prev_sp)
    for peer in peers:
        pl.semaphore_signal(barrier, inc=1, device_id=peer, device_id_type=MESH)
    pl.semaphore_wait(barrier, len(peers))

    def remote(src, dst, send, recv, device):
        return pltpu.make_async_remote_copy(
            src_ref=src,
            dst_ref=dst,
            send_sem=send,
            recv_sem=recv,
            device_id=device,
            device_id_type=MESH,
        )

    sent = []

    def send_x(src, slot, half, device):
        copy = remote(src, xg.at[slot, half], xg_send.at[len(sent)], xg_recv.at[slot, half], device)
        copy.start()
        sent.append(copy)

    def got_x(slot, half):
        remote(
            xg.at[slot, half],
            xg.at[slot, half],
            xg_send.at[0],
            xg_recv.at[slot, half],
            partner,
        ).wait_recv()

    def own(half):
        return normed.at[pl.ds(16 * half, 16)]

    send_x(own(0), tp, 0, x_right)
    send_x(own(1), tp, 1, x_left)
    send_x(own(1), tp, 1, x_right)
    send_x(own(0), tp, 0, x_left)
    send_x(own(0), tp, 0, partner)
    send_x(own(1), tp, 1, partner)
    for half in range(2):
        xg[tp, half] = normed[pl.ds(16 * half, 16), :]
    from_left, from_right, from_far = 2 * xl + core, 2 * xr + core, 2 * x2 + core
    got_x(from_left, 0)
    send_x(xg.at[from_left, 0], from_left, 0, x_right)
    got_x(from_right, 1)
    send_x(xg.at[from_right, 1], from_right, 1, x_left)
    send_x(xg.at[from_left, 0], from_left, 0, partner)
    send_x(xg.at[from_right, 1], from_right, 1, partner)
    got_x(from_left, 1)
    send_x(xg.at[from_left, 1], from_left, 1, partner)
    got_x(from_right, 0)
    send_x(xg.at[from_right, 0], from_right, 0, partner)
    got_x(from_far, 0)
    send_x(xg.at[from_far, 0], from_far, 0, partner)
    got_x(from_far, 1)
    send_x(xg.at[from_far, 1], from_far, 1, partner)

    for j in range(Y):
        for c in range(2):
            m_s[j, c] = jnp.full((256, 128), NEG, F32)
            l_s[j, c] = jnp.zeros((256, 128), F32)
            acc[j, c] = jnp.zeros((256, 256), F32)

    for xx in range(X):
        for half in range(2):
            got_x(2 * xx + 1 - core, half)

    def project(weight):
        rows = xg[...].reshape(256, 2048)
        return jnp.dot(rows, weight[...], preferred_element_type=F32).astype(BF16)

    def kv_send(which, slot, hop, up):
        ref = (k_all, v_all)[which]
        sems = up_send if up else dn_send
        recv = kv_up_recv if up else kv_dn_recv
        return remote(
            ref.at[slot],
            ref.at[slot],
            sems.at[hop, which],
            recv.at[slot, which],
            z_up if up else z_down,
        )

    goes_up = z < zn - 1
    goes_down = z < dn_hops

    def kv_first(which):
        @pl.when(goes_up)
        def _():
            kv_send(which, z, 0, True).start()

        @pl.when(goes_down)
        def _():
            kv_send(which, z, 0, False).start()

    weights[0].wait()
    k_all[z] = project(wk)
    kv_first(0)
    weights[1].wait()
    v_all[z] = project(wv)
    kv_first(1)

    q_sent = []

    def send_q(slot, half, device):
        copy = remote(
            q_all.at[slot, half],
            q_all.at[slot, half],
            q_send.at[len(q_sent)],
            q_recv.at[slot, half],
            device,
        )
        copy.start()
        q_sent.append(copy)

    def got_q(slot, half):
        remote(
            q_all.at[slot, half],
            q_all.at[slot, half],
            q_send.at[0],
            q_recv.at[slot, half],
            y_right,
        ).wait_recv()

    weights[2].wait()
    q_all[y] = project(wq).reshape(2, 128, 256)
    send_q(y, 0, y_right)
    send_q(y, 1, y_left)
    send_q(y, 1, y_right)
    send_q(y, 0, y_left)
    weights[3].wait()
    pin[...] = project(wp)
    halo = remote(pin.at[pl.ds(240, 16)], rim, h_sem.at[0], h_sem.at[1], next_sp)
    halo.start()

    factor = 128 ** (-0.5) * math.log2(math.e)

    def attend(j, slot, masked):
        for c in range(2):
            cols = slice(128 * c, 128 * c + 128)
            q = q_all[j].reshape(256, 256)[:, cols]
            k = k_all[slot, :, cols]
            s = lax.dot_general(q, k, (((1,), (1,)), ((), ())), preferred_element_type=F32) * factor
            if masked:
                row = lax.broadcasted_iota(jnp.int32, (256, 256), 0)
                col = lax.broadcasted_iota(jnp.int32, (256, 256), 1)
                s = jnp.where(col <= row, s, NEG)
            before = m_s[j, c]
            peak = jnp.maximum(before, jnp.max(s, axis=1, keepdims=True))
            shrink = jnp.exp2(before - peak)
            p = jnp.exp2(s - jnp.concatenate([peak, peak], axis=1))
            m_s[j, c] = peak
            l_s[j, c] = l_s[j, c] * shrink + jnp.sum(p, axis=1, keepdims=True)
            pv = jnp.dot(p.astype(BF16), v_all[slot], preferred_element_type=F32)
            acc[j, c] = acc[j, c] * jnp.concatenate([shrink, shrink], axis=1) + pv

    def attend_all(slot):
        def body(j, carry):
            attend(j, slot, False)
            return carry

        lax.fori_loop(0, Y, body, 0)

    attend(y, z, True)

    got_q(yl, 0)
    send_q(yl, 0, y_right)
    got_q(yr, 1)
    send_q(yr, 1, y_left)

    halo.wait()
    ext[pl.ds(0, 16), :] = jnp.where(sp > 0, rim[...].astype(F32), 0.0)
    ext[pl.ds(16, 256), :] = pin[...].astype(F32)
    width = jnp.left_shift(jnp.int32(2), tp % 4)
    window = jnp.zeros((256, 128), F32)
    for offset in range(16):
        window = window + jnp.where(offset < width, ext[pl.ds(16 - offset, 256), :], 0.0)
    position = sp * 256 + lax.broadcasted_iota(jnp.int32, (256, 128), 0)
    counts = jnp.minimum(position + 1, width).astype(F32)
    spread = (window / counts - ext[pl.ds(16, 256), :]).astype(BF16)
    pool_out = jnp.dot(spread, pool_weight[0], preferred_element_type=F32).astype(BF16)
    weights[4].wait()
    for n in range(8):
        cols = slice(256 * n, 256 * n + 256)
        pool_part[:, cols] = jnp.dot(pool_out, pow_[:, cols], preferred_element_type=F32)
    weights[5].wait()

    got_q(yl, 1)
    got_q(yr, 0)
    got_q(y2, 0)
    got_q(y2, 1)

    def own_step(j, carry):
        @pl.when(j > y)
        def _():
            attend(j, z, False)

        return carry

    lax.fori_loop(0, Y, own_step, 0)

    def ring_step(s, carry):
        up_block = jnp.maximum(z - s, 0)
        up_here = s <= z
        up_on = jnp.logical_and(up_here, jnp.logical_and(s < up_hops, z < zn - 1))
        dn_block = (z + s) % zn
        dn_here = jnp.logical_and(s <= dn_hops, dn_block < dn_hops)
        dn_on = jnp.logical_and(dn_here, s < dn_hops)
        dn_used = jnp.logical_and(dn_here, z + s >= zn)
        for which in range(2):

            @pl.when(up_here)
            def _():
                kv_send(which, up_block, 0, True).wait_recv()

            @pl.when(up_on)
            def _():
                kv_send(which, up_block, s, True).start()

            @pl.when(dn_here)
            def _():
                kv_send(which, dn_block, 0, False).wait_recv()

            @pl.when(dn_on)
            def _():
                kv_send(which, dn_block, s, False).start()

        @pl.when(up_here)
        def _():
            attend_all(up_block)

        @pl.when(dn_used)
        def _():
            attend_all(dn_block)

        return carry

    lax.fori_loop(1, up_hops + 1, ring_step, 0)

    def state(j, half):
        rows = pl.ds(128 * half, 128)
        return [(m_s[j, c, rows, :], l_s[j, c, rows, :], acc[j, c, rows, :]) for c in range(2)]

    def arrived(payload, stats):
        columns = jnp.concatenate([stats[...], jnp.zeros((120, 128), F32)], axis=0).T
        return [
            (
                jnp.broadcast_to(columns[:, 2 * c : 2 * c + 1], (128, 128)),
                jnp.broadcast_to(columns[:, 2 * c + 1 : 2 * c + 2], (128, 128)),
                payload[:, 256 * c : 256 * c + 256].astype(F32),
            )
            for c in range(2)
        ]

    def joined(first, second):
        result = []
        for (m1, l1, a1), (m2, l2, a2) in zip(first, second):
            peak = jnp.maximum(m1, m2)
            s1, s2 = jnp.exp2(m1 - peak), jnp.exp2(m2 - peak)
            wide1 = jnp.concatenate([s1, s1], axis=1)
            wide2 = jnp.concatenate([s2, s2], axis=1)
            result.append((peak, l1 * s1 + l2 * s2, a1 * wide1 + a2 * wide2))
        return result

    y_sent = []

    def send_state(values, index, payload, stats, device):
        (m0, l0, a0), (m1, l1, a1) = values
        lane = lax.broadcasted_iota(jnp.int32, (128, 128), 1)
        table = jnp.where(lane == 0, m0, jnp.where(lane == 1, l0, jnp.where(lane == 2, m1, l1)))
        pst[index] = table.T[:8]
        ps[index, :, :256] = a0.astype(BF16)
        ps[index, :, 256:] = a1.astype(BF16)
        for i, (src, dst) in enumerate(((ps, payload), (pst, stats))):
            copy = remote(src.at[index], dst, ps_send.at[index, i], ps_recv.at[index, i], device)
            copy.start()
            y_sent.append(copy)

    def got_state(index, payload, stats):
        for i, (src, dst) in enumerate(((ps, payload), (pst, stats))):
            remote(
                src.at[index], dst, ps_send.at[index, i], ps_recv.at[index, i], y_right
            ).wait_recv()

    send_state(state(y2, 0), 0, r2.at[0], r2t.at[0], y_right)
    send_state(state(y2, 1), 1, r2.at[1], r2t.at[1], y_left)
    send_state(state(yr, 1), 2, rn.at[0, 1], rnt.at[0, 1], y_right)
    send_state(state(yl, 0), 3, rn.at[1, 0], rnt.at[1, 0], y_left)
    got_state(0, r2.at[0], r2t.at[0])
    send_state(
        joined(state(yr, 0), arrived(r2.at[0], r2t.at[0])), 4, rn.at[0, 0], rnt.at[0, 0], y_right
    )
    got_state(1, r2.at[1], r2t.at[1])
    send_state(
        joined(state(yl, 1), arrived(r2.at[1], r2t.at[1])), 5, rn.at[1, 1], rnt.at[1, 1], y_left
    )
    level = balance[tp]
    got_state(2, rn.at[0, 1], rnt.at[0, 1])
    got_state(3, rn.at[1, 0], rnt.at[1, 0])
    for half in range(2):
        if half == 0:
            got_state(4, rn.at[0, 0], rnt.at[0, 0])
        else:
            got_state(5, rn.at[1, 1], rnt.at[1, 1])
        whole = state(y, half)
        for side in range(2):
            whole = joined(whole, arrived(rn.at[side, half], rnt.at[side, half]))
        maps = [
            (a / jnp.concatenate([l, l], axis=1)).astype(BF16).astype(F32) for _, l, a in whole
        ]
        contrast = maps[0] - level * maps[1]
        square = jnp.mean(contrast * contrast, axis=1, keepdims=True)
        contrast = contrast * lax.rsqrt(square + norm_epsilon) * gain[...]
        co[pl.ds(128 * half, 128), :] = contrast.astype(BF16)

    mixed = co[...]
    for n in range(8):
        cols = slice(256 * n, 256 * n + 256)
        tile = jnp.dot(mixed, cow[:, cols], preferred_element_type=F32) + pool_part[:, cols]
        part[:, :, :, :, cols] = tile.astype(BF16).reshape(X, 2, 2, 16, 256)
    pair = [
        remote(part.at[xx, 1 - core], pr.at[xx], pr_send.at[xx], pr_recv.at[xx], partner)
        for xx in range(X)
    ]
    for copy in pair:
        copy.start()
    for copy in pair:
        copy.wait_recv()

    def both(owner, half):
        return part[owner, core, half].astype(F32) + pr[owner, half].astype(F32)

    x_sent = []

    def send_sum(value, index, dst, device):
        xs[index] = value.astype(BF16)
        copy = remote(xs.at[index], dst, xs_send.at[index], xs_recv.at[index], device)
        copy.start()
        x_sent.append(copy)

    def got_sum(index, dst):
        remote(xs.at[index], dst, xs_send.at[index], xs_recv.at[index], x_right).wait_recv()

    send_sum(both(x2, 0), 0, xr2.at[0], x_right)
    send_sum(both(x2, 1), 1, xr2.at[1], x_left)
    send_sum(both(xr, 1), 2, xrn.at[0, 1], x_right)
    send_sum(both(xl, 0), 3, xrn.at[1, 0], x_left)
    got_sum(0, xr2.at[0])
    send_sum(both(xr, 0) + xr2[0].astype(F32), 4, xrn.at[0, 0], x_right)
    got_sum(1, xr2.at[1])
    send_sum(both(xl, 1) + xr2[1].astype(F32), 5, xrn.at[1, 1], x_left)
    got_sum(2, xrn.at[0, 1])
    got_sum(3, xrn.at[1, 0])
    got_sum(4, xrn.at[0, 0])
    got_sum(5, xrn.at[1, 1])
    for half in range(2):
        total = both(x, half) + xrn[0, half].astype(F32) + xrn[1, half].astype(F32)
        out[pl.ds(16 * half, 16), :] = total.astype(BF16)

    for copy in sent + q_sent + y_sent + pair + x_sent:
        copy.wait_send()

    def drain(s, carry):
        up_on = jnp.logical_and(s <= z, goes_up)
        dn_on = (z + s) % zn < dn_hops
        for which in range(2):

            @pl.when(up_on)
            def _():
                kv_send(which, jnp.maximum(z - s, 0), s, True).wait_send()

            @pl.when(jnp.logical_and(dn_on, s < dn_hops))
            def _():
                kv_send(which, (z + s) % zn, s, False).wait_send()

        return carry

    lax.fori_loop(0, up_hops, drain, 0)


def solution(mesh):
    zn = mesh.shape["sp"] // Y

    def per_device(
        normed,
        query_weight,
        key_weight,
        value_weight,
        pool_in_weight,
        pool_weight,
        map_balance,
        head_gain,
        contrast_out_weight,
        pool_out_weight,
    ):
        vmem = pl.BlockSpec(memory_space=pltpu.VMEM)
        hbm = pl.BlockSpec(memory_space=pl.ANY)
        smem = pl.BlockSpec(memory_space=pltpu.SMEM)
        dma = pltpu.SemaphoreType.DMA
        V = pltpu.VMEM
        return pl.pallas_call(
            functools.partial(kernel, zn),
            out_shape=jax.ShapeDtypeStruct(normed.shape, BF16),
            in_specs=[vmem, hbm, hbm, hbm, hbm, vmem, smem, vmem, hbm, hbm],
            out_specs=vmem,
            scratch_shapes=[
                V((8, 2, 16, 2048), BF16),
                V((2048, 256), BF16),
                V((2048, 256), BF16),
                V((2048, 256), BF16),
                V((2048, 128), BF16),
                V((256, 2048), BF16),
                V((128, 2048), BF16),
                V((Y, 2, 128, 256), BF16),
                V((zn, 256, 256), BF16),
                V((zn, 256, 256), BF16),
                V((Y, 2, 256, 256), F32),
                V((Y, 2, 256, 128), F32),
                V((Y, 2, 256, 128), F32),
                V((256, 128), BF16),
                V((16, 128), BF16),
                V((272, 128), F32),
                V((256, 2048), F32),
                V((6, 128, 512), BF16),
                V((6, 8, 128), F32),
                V((2, 128, 512), BF16),
                V((2, 8, 128), F32),
                V((2, 2, 128, 512), BF16),
                V((2, 2, 8, 128), F32),
                V((256, 256), BF16),
                V((X, 2, 2, 16, 2048), BF16),
                V((X, 2, 16, 2048), BF16),
                V((6, 16, 2048), BF16),
                V((2, 16, 2048), BF16),
                V((2, 2, 16, 2048), BF16),
                dma((6,)),
                dma((14,)),
                dma((8, 2)),
                dma((zn // 2, 2)),
                dma((zn // 2, 2)),
                dma((zn, 2)),
                dma((zn, 2)),
                dma((6,)),
                dma((Y, 2)),
                dma((2,)),
                dma((6, 2)),
                dma((6, 2)),
                dma((X,)),
                dma((X,)),
                dma((6,)),
                dma((6,)),
            ],
            compiler_params=pltpu.CompilerParams(
                collective_id=0, has_side_effects=True, vmem_limit_bytes=50 * 1024 * 1024
            ),
        )(
            normed,
            query_weight,
            key_weight,
            value_weight,
            pool_in_weight,
            pool_weight,
            map_balance,
            head_gain.reshape(1, -1),
            contrast_out_weight,
            pool_out_weight,
        )

    return jax.shard_map(
        per_device,
        mesh=mesh,
        in_specs=(
            P(("sp", "tp"), None),
            P(None, "tp"),
            P(None, "tp"),
            P(None, "tp"),
            P(None, "tp"),
            P("tp", None, None),
            P(),
            P(),
            P("tp", None),
            P("tp", None),
        ),
        out_specs=P(("sp", "tp"), None),
        check_vma=False,
    )
```

time: 308 us -> 98.9 us (0.32)
  the two profiles are of different devices: /device:TPU:448 before, /device:TPU:385 now
where the time goes in v1:
time: 98.9 us; the launch traced here: 98.5 us
  Pallas kernels  91 us (92%)
  local copies, waits for them, and re-layouts  7.53 us (8%)
    pallas_call x1, Pallas kernels, per_device(): pl.pallas_call(functools.partial(kernel, zn), out_shape=jax.ShapeDtypeStr...  91 us
    unnamed x17, local copies, waits for them, and re-layouts  7.53 us

profile of v1, /device:TPU:385, one launch (start us, length us, event | category | flops | bytes accessed | tf_op | source)
XLA Modules:
  0.0 98.5 jit_solution(14739165142696980654)
XLA Ops:
  0.0 0.0 copy-start.6
  0.0 0.0 copy-start.7
  0.0 0.7 copy-done.6
  0.7 0.0 copy-done.7
  0.7 0.0 copy-start
  0.7 1.2 %copy-done = bf16[2048,256]{1,0:T(8,128)(2,1)S(1)} copy-done((bf16[2048,256]{1,0:T(8,128)(2,1)S(1)}, bf16[2048,256]{1,0:T(8,128)(2,1)}, u32[]{:S(2)}) %copy-start) | copy-done | bytes 1048600
  1.9 0.0 copy-start.1
  1.9 1.2 %copy-done.1 = bf16[2048,256]{1,0:T(8,128)(2,1)S(1)} copy-done((bf16[2048,256]{1,0:T(8,128)(2,1)S(1)}, bf16[2048,256]{1,0:T(8,128)(2,1)}, u32[]{:S(2)}) %copy-start.1) | copy-done | bytes 1048600
  3.1 0.0 copy-start.2
  3.1 1.0 %copy-done.2 = bf16[2048,128]{1,0:T(8,128)(2,1)S(1)} copy-done((bf16[2048,128]{1,0:T(8,128)(2,1)S(1)}, bf16[2048,128]{1,0:T(8,128)(2,1)}, u32[]{:S(2)}) %copy-start.2) | copy-done | bytes 524312
  4.2 0.0 copy-start.3
  4.2 1.0 %copy-done.3 = bf16[128,2048]{1,0:T(8,128)(2,1)S(1)} copy-done((bf16[128,2048]{1,0:T(8,128)(2,1)S(1)}, bf16[128,2048]{1,0:T(8,128)(2,1)}, u32[]{:S(2)}) %copy-start.3) | copy-done | bytes 524312
  5.2 0.0 copy-start.4
  5.2 0.9 copy-done.4
  6.1 0.0 copy-start.5
  6.1 0.8 copy-done.5
  6.9 91.0 %shard_map.100 = bf16[32,2048]{1,0:T(8,128)(2,1)S(1)} custom-call(bf16[32,2048]{1,0:T(8,128)(2,1)S(1)} %copy-done.4, bf16[2048,256]{1,0:T(8,128)(2,1)S(1)} %copy-done, bf16[2048,256]{1,0:T(8,128)(2,1)S(1)} %copy-done.1, bf16[2048,256]{1,0:T(8,128)(2,1)} %wv_h.1, bf16[2048,128]{1,0:T(8,128)(2,1)S(1)} %copy-done.2, bf16[1,128,128]{2,1,0:T(8,128)(2,1)S(1)} %copy-done.5, ...), custom_call_target="tpu_custom_call" | custom-call | tf_op jit(solution)/shard_map/pallas_call | solution.py:513
  97.8 0.7 copy.12
Async XLA Ops:
  0.0 0.7 copy-start.6
  0.0 0.7 copy-start.7
  0.7 1.2 %copy-start = (bf16[2048,256]{1,0:T(8,128)(2,1)S(1)}, bf16[2048,256]{1,0:T(8,128)(2,1)}, u32[]{:S(2)}) copy-start(bf16[2048,256]{1,0:T(8,128)(2,1)} %wq_h.1) | copy-start | bytes 3145732
  1.9 1.2 %copy-start.1 = (bf16[2048,256]{1,0:T(8,128)(2,1)S(1)}, bf16[2048,256]{1,0:T(8,128)(2,1)}, u32[]{:S(2)}) copy-start(bf16[2048,256]{1,0:T(8,128)(2,1)} %wk_h.1) | copy-start | bytes 3145732
  3.1 1.0 %copy-start.2 = (bf16[2048,128]{1,0:T(8,128)(2,1)S(1)}, bf16[2048,128]{1,0:T(8,128)(2,1)}, u32[]{:S(2)}) copy-start(bf16[2048,128]{1,0:T(8,128)(2,1)} %wp_h.1) | copy-start | bytes 1572868
  4.2 1.0 %copy-start.3 = (bf16[128,2048]{1,0:T(8,128)(2,1)S(1)}, bf16[128,2048]{1,0:T(8,128)(2,1)}, u32[]{:S(2)}) copy-start(bf16[128,2048]{1,0:T(8,128)(2,1)} %pow_h.1) | copy-start | bytes 1572868
  5.2 0.9 copy-start.4
  6.1 0.8 copy-start.5

commit v2 on v1

--- a/solution.py
+++ b/solution.py
@@ -19,27 +19,28 @@
 
 def kernel(
     zn,
-    normed,
+    normed_h,
     wq_h,
     wk_h,
     wv_h,
     wp_h,
-    pool_weight,
-    balance,
-    gain,
+    pool_weight_h,
+    balance_h,
+    gain_h,
     cow_h,
     pow_h,
     out,
     xg,
+    wkv,
     wq,
-    wk,
-    wv,
     wp,
     cow,
     pow_,
+    pool_weight,
+    gain,
+    balance,
     q_all,
-    k_all,
-    v_all,
+    kv_all,
     acc,
     m_s,
     l_s,
@@ -81,8 +82,7 @@
     nsp = zn * Y
     z, y = sp // Y, sp % Y
     x, core = tp // 2, tp % 2
-    up_hops = zn // 2
-    dn_hops = zn // 2 - 1
+    hops = zn // 2
 
     def at(zz, yy, xx, cc):
         return {"sp": zz * Y + yy, "tp": xx * 2 + cc}
@@ -102,17 +102,34 @@
     weights = [
         pltpu.make_async_copy(src, dst, w_sem.at[i])
         for i, (src, dst) in enumerate(
-            ((wk_h, wk), (wv_h, wv), (wq_h, wq), (wp_h, wp), (pow_h, pow_), (cow_h, cow))
+            (
+                (wk_h, wkv.at[:, pl.ds(0, 256)]),
+                (wv_h, wkv.at[:, pl.ds(256, 256)]),
+                (wq_h, wq),
+                (wp_h, wp),
+                (pow_h, pow_),
+                (cow_h, cow),
+                (pool_weight_h, pool_weight),
+                (gain_h, gain),
+                (balance_h, balance),
+            )
         )
     ]
-    for copy in weights:
+    rows_in = [
+        pltpu.make_async_copy(
+            normed_h.at[pl.ds(16 * half, 16)], xg.at[tp, half], w_sem.at[len(weights) + half]
+        )
+        for half in range(2)
+    ]
+    for copy in rows_in + weights:
         copy.start()
-
     barrier = pltpu.get_barrier_semaphore()
     peers = (partner, x_right, x_left, y_right, y_left, z_up, z_down, next_sp, prev_sp)
     for peer in peers:
         pl.semaphore_signal(barrier, inc=1, device_id=peer, device_id_type=MESH)
     pl.semaphore_wait(barrier, len(peers))
+    for copy in rows_in:
+        copy.wait()
 
     def remote(src, dst, send, recv, device):
         return pltpu.make_async_remote_copy(
@@ -123,7 +140,6 @@
             device_id=device,
             device_id_type=MESH,
         )
-
     sent = []
 
     def send_x(src, slot, half, device):
@@ -141,17 +157,90 @@
         ).wait_recv()
 
     def own(half):
-        return normed.at[pl.ds(16 * half, 16)]
+        return xg.at[tp, half]
 
     send_x(own(0), tp, 0, x_right)
     send_x(own(1), tp, 1, x_left)
+    send_x(own(0), tp, 0, partner)
+    send_x(own(1), tp, 1, partner)
     send_x(own(1), tp, 1, x_right)
     send_x(own(0), tp, 0, x_left)
-    send_x(own(0), tp, 0, partner)
-    send_x(own(1), tp, 1, partner)
-    for half in range(2):
-        xg[tp, half] = normed[pl.ds(16 * half, 16), :]
+
+    order = (x, xl, xr, x2)
+
+    def kv_copy(slot, i, hop, up):
+        piece = kv_all.at[slot, order[i]]
+        return remote(
+            piece,
+            piece,
+            (up_send if up else dn_send).at[hop, i],
+            (kv_up_recv if up else kv_dn_recv).at[slot, i],
+            z_up if up else z_down,
+        )
+
+    def sends(s, i):
+        up = jnp.logical_and(s <= z, z < zn - 1)
+        up = jnp.logical_and(up, s + 1 <= (hops if i < 2 else hops - 1))
+        dn = (z + s) % zn <= (hops - 1 if i >= 2 else hops - 2)
+        dn = jnp.logical_and(dn, s + 1 <= (hops if i >= 2 else hops - 1))
+        return up, dn
+
+    def kv_start(s, i):
+        up, dn = sends(s, i)
+
+        @pl.when(up)
+        def _():
+            kv_copy(jnp.maximum(z - s, 0), i, s, True).start()
+
+        @pl.when(dn)
+        def _():
+            kv_copy((z + s) % zn, i, s, False).start()
+
+    def pass_on(s, i):
+        up_here = jnp.logical_and(s <= z, s <= (hops if i < 2 else hops - 1))
+        dn_here = (z + s) % zn <= (hops - 1 if i >= 2 else hops - 2)
+        dn_here = jnp.logical_and(dn_here, s <= (hops if i >= 2 else hops - 1))
+        up, dn = sends(s, i)
+
+        @pl.when(up_here)
+        def _():
+            kv_copy(jnp.maximum(z - s, 0), i, 0, True).wait_recv()
+
+        @pl.when(up)
+        def _():
+            kv_copy(jnp.maximum(z - s, 0), i, s, True).start()
+
+        @pl.when(dn_here)
+        def _():
+            kv_copy((z + s) % zn, i, 0, False).wait_recv()
+
+        @pl.when(dn)
+        def _():
+            kv_copy((z + s) % zn, i, s, False).start()
+
+    def project(rows, weight):
+        return jnp.dot(rows, weight[...], preferred_element_type=F32).astype(BF16)
+
+    def project_kv(i):
+        chip = order[i]
+        rows = xg[pl.ds(2 * chip, 2)].reshape(64, 2048)
+        kv_all[z, chip] = project(rows, wkv)
+        kv_start(0, i)
+
     from_left, from_right, from_far = 2 * xl + core, 2 * xr + core, 2 * x2 + core
+
+    def got_chip(chip):
+        for half in range(2):
+            got_x(2 * chip + 1 - core, half)
+    for j in range(Y):
+        for c in range(2):
+            m_s[j, c] = jnp.full((256, 128), NEG, F32)
+            l_s[j, c] = jnp.zeros((256, 128), F32)
+            acc[j, c] = jnp.zeros((256, 256), F32)
+    weights[0].wait()
+    weights[1].wait()
+    got_chip(x)
+    project_kv(0)
     got_x(from_left, 0)
     send_x(xg.at[from_left, 0], from_left, 0, x_right)
     got_x(from_right, 1)
@@ -162,55 +251,16 @@
     send_x(xg.at[from_left, 1], from_left, 1, partner)
     got_x(from_right, 0)
     send_x(xg.at[from_right, 0], from_right, 0, partner)
+    got_chip(xl)
+    project_kv(1)
     got_x(from_far, 0)
     send_x(xg.at[from_far, 0], from_far, 0, partner)
     got_x(from_far, 1)
     send_x(xg.at[from_far, 1], from_far, 1, partner)
-
-    for j in range(Y):
-        for c in range(2):
-            m_s[j, c] = jnp.full((256, 128), NEG, F32)
-            l_s[j, c] = jnp.zeros((256, 128), F32)
-            acc[j, c] = jnp.zeros((256, 256), F32)
-
-    for xx in range(X):
-        for half in range(2):
-            got_x(2 * xx + 1 - core, half)
-
-    def project(weight):
-        rows = xg[...].reshape(256, 2048)
-        return jnp.dot(rows, weight[...], preferred_element_type=F32).astype(BF16)
-
-    def kv_send(which, slot, hop, up):
-        ref = (k_all, v_all)[which]
-        sems = up_send if up else dn_send
-        recv = kv_up_recv if up else kv_dn_recv
-        return remote(
-            ref.at[slot],
-            ref.at[slot],
-            sems.at[hop, which],
-            recv.at[slot, which],
-            z_up if up else z_down,
-        )
-
-    goes_up = z < zn - 1
-    goes_down = z < dn_hops
-
-    def kv_first(which):
-        @pl.when(goes_up)
-        def _():
-            kv_send(which, z, 0, True).start()
-
-        @pl.when(goes_down)
-        def _():
-            kv_send(which, z, 0, False).start()
-
-    weights[0].wait()
-    k_all[z] = project(wk)
-    kv_first(0)
-    weights[1].wait()
-    v_all[z] = project(wv)
-    kv_first(1)
+    got_chip(xr)
+    project_kv(2)
+    got_chip(x2)
+    project_kv(3)
 
     q_sent = []
 
@@ -233,25 +283,25 @@
             q_recv.at[slot, half],
             y_right,
         ).wait_recv()
-
     weights[2].wait()
-    q_all[y] = project(wq).reshape(2, 128, 256)
+    whole_rows = xg[...].reshape(256, 2048)
+    q_all[y] = project(whole_rows, wq).reshape(2, 128, 256)
     send_q(y, 0, y_right)
     send_q(y, 1, y_left)
     send_q(y, 1, y_right)
     send_q(y, 0, y_left)
     weights[3].wait()
-    pin[...] = project(wp)
+    pin[...] = project(whole_rows, wp)
     halo = remote(pin.at[pl.ds(240, 16)], rim, h_sem.at[0], h_sem.at[1], next_sp)
     halo.start()
-
     factor = 128 ** (-0.5) * math.log2(math.e)
 
     def attend(j, slot, masked):
         for c in range(2):
             cols = slice(128 * c, 128 * c + 128)
             q = q_all[j].reshape(256, 256)[:, cols]
-            k = k_all[slot, :, cols]
+            k = kv_all[slot].reshape(256, 512)[:, cols]
+            v = kv_all[slot].reshape(256, 512)[:, 256:]
             s = lax.dot_general(q, k, (((1,), (1,)), ((), ())), preferred_element_type=F32) * factor
             if masked:
                 row = lax.broadcasted_iota(jnp.int32, (256, 256), 0)
@@ -263,23 +313,39 @@
             p = jnp.exp2(s - jnp.concatenate([peak, peak], axis=1))
             m_s[j, c] = peak
             l_s[j, c] = l_s[j, c] * shrink + jnp.sum(p, axis=1, keepdims=True)
-            pv = jnp.dot(p.astype(BF16), v_all[slot], preferred_element_type=F32)
+            pv = jnp.dot(p.astype(BF16), v, preferred_element_type=F32)
             acc[j, c] = acc[j, c] * jnp.concatenate([shrink, shrink], axis=1) + pv
 
-    def attend_all(slot):
-        def body(j, carry):
+    def work(u):
+        first = u < Y
+        s = (u - Y) // 8 + 1
+        k = jnp.where(first, u, (u - Y) % 8)
+        up = k < Y
+        near = k % Y
+        j = (y + jnp.where(near == 3, 0, jnp.where(near == 2, 3, 2 - near))) % Y
+        slot = jnp.where(first, z, jnp.where(up, jnp.maximum(z - s, 0), (z + s) % zn))
+        below = jnp.logical_and(up, s <= z)
+        above = jnp.logical_and(z + s >= zn, jnp.logical_and(s < hops, jnp.logical_not(up)))
+        wanted = jnp.where(first, j > y, jnp.logical_or(below, above))
+
+        @pl.when(wanted)
+        def _():
             attend(j, slot, False)
+
+    def work_until(done, ready, most):
+        count = jnp.minimum(ready - done, most)
+
+        def one(i, carry):
+            work(done + i)
             return carry
 
-        lax.fori_loop(0, Y, body, 0)
-
+        lax.fori_loop(0, count, one, 0)
+        return done + count
+
+    pass_on(1, 0)
+    pass_on(1, 1)
     attend(y, z, True)
-
-    got_q(yl, 0)
-    send_q(yl, 0, y_right)
-    got_q(yr, 1)
-    send_q(yr, 1, y_left)
-
+    pass_on(1, 2)
     halo.wait()
     ext[pl.ds(0, 16), :] = jnp.where(sp > 0, rim[...].astype(F32), 0.0)
     ext[pl.ds(16, 256), :] = pin[...].astype(F32)
@@ -290,65 +356,45 @@
     position = sp * 256 + lax.broadcasted_iota(jnp.int32, (256, 128), 0)
     counts = jnp.minimum(position + 1, width).astype(F32)
     spread = (window / counts - ext[pl.ds(16, 256), :]).astype(BF16)
+    weights[6].wait()
     pool_out = jnp.dot(spread, pool_weight[0], preferred_element_type=F32).astype(BF16)
     weights[4].wait()
     for n in range(8):
         cols = slice(256 * n, 256 * n + 256)
         pool_part[:, cols] = jnp.dot(pool_out, pow_[:, cols], preferred_element_type=F32)
-    weights[5].wait()
-
+    for copy in weights[5:]:
+        if copy is not weights[6]:
+            copy.wait()
+    pass_on(1, 3)
+    got_q(yl, 0)
+    send_q(yl, 0, y_right)
+    got_q(yr, 1)
+    send_q(yr, 1, y_left)
+    pass_on(2, 0)
     got_q(yl, 1)
     got_q(yr, 0)
+    pass_on(2, 1)
     got_q(y2, 0)
     got_q(y2, 1)
-
-    def own_step(j, carry):
-        @pl.when(j > y)
-        def _():
-            attend(j, z, False)
-
-        return carry
-
-    lax.fori_loop(0, Y, own_step, 0)
-
-    def ring_step(s, carry):
-        up_block = jnp.maximum(z - s, 0)
-        up_here = s <= z
-        up_on = jnp.logical_and(up_here, jnp.logical_and(s < up_hops, z < zn - 1))
-        dn_block = (z + s) % zn
-        dn_here = jnp.logical_and(s <= dn_hops, dn_block < dn_hops)
-        dn_on = jnp.logical_and(dn_here, s < dn_hops)
-        dn_used = jnp.logical_and(dn_here, z + s >= zn)
-        for which in range(2):
-
-            @pl.when(up_here)
-            def _():
-                kv_send(which, up_block, 0, True).wait_recv()
-
-            @pl.when(up_on)
-            def _():
-                kv_send(which, up_block, s, True).start()
-
-            @pl.when(dn_here)
-            def _():
-                kv_send(which, dn_block, 0, False).wait_recv()
-
-            @pl.when(dn_on)
-            def _():
-                kv_send(which, dn_block, s, False).start()
-
-        @pl.when(up_here)
-        def _():
-            attend_all(up_block)
-
-        @pl.when(dn_used)
-        def _():
-            attend_all(dn_block)
-
-        return carry
-
-    lax.fori_loop(1, up_hops + 1, ring_step, 0)
-
+    done = work_until(0, 4 + 8, 3)
+    pass_on(2, 2)
+    done = work_until(done, 4 + 8, 3)
+    pass_on(2, 3)
+    done = work_until(done, 4 + 16, 3)
+
+    def ring_step(s, done):
+        for i in range(4):
+            pass_on(s, i)
+            done = work_until(done, Y + 8 * (s if i == 3 else s - 1), 3)
+        return done
+
+    done = lax.fori_loop(3, hops, ring_step, done)
+    pass_on(hops, 0)
+    pass_on(hops, 2)
+    done = work_until(done, Y + 8 * (hops - 1), 3)
+    pass_on(hops, 1)
+    pass_on(hops, 3)
+    work_until(done, Y + 8 * (hops - 1), 99)
     def state(j, half):
         rows = pl.ds(128 * half, 128)
         return [(m_s[j, c, rows, :], l_s[j, c, rows, :], acc[j, c, rows, :]) for c in range(2)]
@@ -394,10 +440,15 @@
                 src.at[index], dst, ps_send.at[index, i], ps_recv.at[index, i], y_right
             ).wait_recv()
 
+    base = Y + 8 * (hops - 1)
+    work(base)
     send_state(state(y2, 0), 0, r2.at[0], r2t.at[0], y_right)
     send_state(state(y2, 1), 1, r2.at[1], r2t.at[1], y_left)
+    work(base + 1)
     send_state(state(yr, 1), 2, rn.at[0, 1], rnt.at[0, 1], y_right)
+    work(base + 2)
     send_state(state(yl, 0), 3, rn.at[1, 0], rnt.at[1, 0], y_left)
+    work(base + 3)
     got_state(0, r2.at[0], r2t.at[0])
     send_state(
         joined(state(yr, 0), arrived(r2.at[0], r2t.at[0])), 4, rn.at[0, 0], rnt.at[0, 0], y_right
@@ -424,7 +475,6 @@
         square = jnp.mean(contrast * contrast, axis=1, keepdims=True)
         contrast = contrast * lax.rsqrt(square + norm_epsilon) * gain[...]
         co[pl.ds(128 * half, 128), :] = contrast.astype(BF16)
-
     mixed = co[...]
     for n in range(8):
         cols = slice(256 * n, 256 * n + 256)
@@ -438,7 +488,6 @@
         copy.start()
     for copy in pair:
         copy.wait_recv()
-
     def both(owner, half):
         return part[owner, core, half].astype(F32) + pr[owner, half].astype(F32)
 
@@ -468,26 +517,24 @@
     for half in range(2):
         total = both(x, half) + xrn[0, half].astype(F32) + xrn[1, half].astype(F32)
         out[pl.ds(16 * half, 16), :] = total.astype(BF16)
-
     for copy in sent + q_sent + y_sent + pair + x_sent:
         copy.wait_send()
 
     def drain(s, carry):
-        up_on = jnp.logical_and(s <= z, goes_up)
-        dn_on = (z + s) % zn < dn_hops
-        for which in range(2):
-
-            @pl.when(up_on)
+        for i in range(4):
+            up, dn = sends(s, i)
+
+            @pl.when(up)
             def _():
-                kv_send(which, jnp.maximum(z - s, 0), s, True).wait_send()
-
-            @pl.when(jnp.logical_and(dn_on, s < dn_hops))
+                kv_copy(jnp.maximum(z - s, 0), i, s, True).wait_send()
+
+            @pl.when(dn)
             def _():
-                kv_send(which, (z + s) % zn, s, False).wait_send()
+                kv_copy((z + s) % zn, i, s, False).wait_send()
 
         return carry
 
-    lax.fori_loop(0, up_hops, drain, 0)
+    lax.fori_loop(0, hops, drain, 0)
 
 
 def solution(mesh):
@@ -507,25 +554,25 @@
     ):
         vmem = pl.BlockSpec(memory_space=pltpu.VMEM)
         hbm = pl.BlockSpec(memory_space=pl.ANY)
-        smem = pl.BlockSpec(memory_space=pltpu.SMEM)
         dma = pltpu.SemaphoreType.DMA
         V = pltpu.VMEM
         return pl.pallas_call(
             functools.partial(kernel, zn),
             out_shape=jax.ShapeDtypeStruct(normed.shape, BF16),
-            in_specs=[vmem, hbm, hbm, hbm, hbm, vmem, smem, vmem, hbm, hbm],
+            in_specs=[hbm] * 10,
             out_specs=vmem,
             scratch_shapes=[
                 V((8, 2, 16, 2048), BF16),
-                V((2048, 256), BF16),
-                V((2048, 256), BF16),
+                V((2048, 512), BF16),
                 V((2048, 256), BF16),
                 V((2048, 128), BF16),
                 V((256, 2048), BF16),
                 V((128, 2048), BF16),
+                V((1, 128, 128), BF16),
+                V((1, 256), F32),
+                pltpu.SMEM((8,), F32),
                 V((Y, 2, 128, 256), BF16),
-                V((zn, 256, 256), BF16),
-                V((zn, 256, 256), BF16),
+                V((zn, X, 64, 512), BF16),
                 V((Y, 2, 256, 256), F32),
                 V((Y, 2, 256, 128), F32),
                 V((Y, 2, 256, 128), F32),
@@ -545,13 +592,13 @@
                 V((6, 16, 2048), BF16),
                 V((2, 16, 2048), BF16),
                 V((2, 2, 16, 2048), BF16),
-                dma((6,)),
+                dma((11,)),
                 dma((14,)),
                 dma((8, 2)),
-                dma((zn // 2, 2)),
-                dma((zn // 2, 2)),
-                dma((zn, 2)),
-                dma((zn, 2)),
+                dma((zn // 2, X)),
+                dma((zn // 2, X)),
+                dma((zn, X)),
+                dma((zn, X)),
                 dma((6,)),
                 dma((Y, 2)),
                 dma((2,)),
@@ -563,7 +610,7 @@
                 dma((6,)),
             ],
             compiler_params=pltpu.CompilerParams(
-                collective_id=0, has_side_effects=True, vmem_limit_bytes=50 * 1024 * 1024
+                collective_id=0, has_side_effects=True, vmem_limit_bytes=67043328
             ),
         )(
             normed,

time: 98.9 us -> 84.2 us (0.85)
  the two profiles are of different devices: /device:TPU:385 before, /device:TPU:451 now
where the time goes in v2:
time: 84.2 us; the launch traced here: 84.1 us
  Pallas kernels  82.5 us (98%)
  local copies, waits for them, and re-layouts  1.57 us (2%)
    pallas_call x1, Pallas kernels, per_device(): pl.pallas_call(functools.partial(kernel, zn), out_shape=jax.ShapeDtypeStr...  82.5 us

profile of v2, /device:TPU:451, one launch (start us, length us, event | category | flops | bytes accessed | tf_op | source)
XLA Modules:
  0.0 84.1 jit_solution(12277527669740337041)
XLA Ops:
  0.0 82.5 %shard_map.100 = bf16[32,2048]{1,0:T(8,128)(2,1)} custom-call(bf16[32,2048]{1,0:T(8,128)(2,1)} %normed_h.1, bf16[2048,256]{1,0:T(8,128)(2,1)} %wq_h.1, bf16[2048,256]{1,0:T(8,128)(2,1)} %wk_h.1, bf16[2048,256]{1,0:T(8,128)(2,1)} %wv_h.1, bf16[2048,128]{1,0:T(8,128)(2,1)} %wp_h.1, bf16[1,128,128]{2,1,0:T(8,128)(2,1)} %pool_weight_h.1, f32[8]{0:T(128)} %balance_h.1, ...), custom_call_target="tpu_custom_call" | custom-call | tf_op jit(solution)/shard_map/pallas_call | solution.py:559
  82.5 1.6 %copy.12 = bf16[32,2048]{1,0:T(8,128)(2,1)} copy(bf16[32,2048]{1,0:T(8,128)(2,1)} %shard_map.100) | data formatting | bytes 262144

commit v3 on v2

--- a/solution.py
+++ b/solution.py
@@ -65,8 +65,7 @@
     xg_recv,
     up_send,
     dn_send,
-    kv_up_recv,
-    kv_dn_recv,
+    kv_recv,
     q_send,
     q_recv,
     h_sem,
@@ -173,8 +172,8 @@
         return remote(
             piece,
             piece,
-            (up_send if up else dn_send).at[hop, i],
-            (kv_up_recv if up else kv_dn_recv).at[slot, i],
+            (up_send if up else dn_send).at[hop % 2, i],
+            kv_recv.at[slot, i],
             z_up if up else z_down,
         )
 
@@ -185,6 +184,17 @@
         dn = jnp.logical_and(dn, s + 1 <= (hops if i >= 2 else hops - 1))
         return up, dn
 
+    def kv_left(s, i):
+        up, dn = sends(s, i)
+
+        @pl.when(up)
+        def _():
+            kv_copy(jnp.maximum(z - s, 0), i, s, True).wait_send()
+
+        @pl.when(dn)
+        def _():
+            kv_copy((z + s) % zn, i, s, False).wait_send()
+
     def kv_start(s, i):
         up, dn = sends(s, i)
 
@@ -201,6 +211,8 @@
         dn_here = (z + s) % zn <= (hops - 1 if i >= 2 else hops - 2)
         dn_here = jnp.logical_and(dn_here, s <= (hops if i >= 2 else hops - 1))
         up, dn = sends(s, i)
+        if not (isinstance(s, int) and s < 2):
+            kv_left(s - 2, i)
 
         @pl.when(up_here)
         def _():
@@ -226,6 +238,35 @@
         rows = xg[pl.ds(2 * chip, 2)].reshape(64, 2048)
         kv_all[z, chip] = project(rows, wkv)
         kv_start(0, i)
+
+    q_sent = []
+
+    def q_copy(slot, i, device, send):
+        piece = q_all.at[slot, order[i]]
+        return remote(piece, piece, q_send.at[send], q_recv.at[slot, i], device)
+
+    def send_q(slot, i, device):
+        copy = q_copy(slot, i, device, len(q_sent))
+        copy.start()
+        q_sent.append(copy)
+
+    def got_q(slot, i):
+        q_copy(slot, i, y_right, 0).wait_recv()
+
+    def project_q(i):
+        chip = order[i]
+        rows = xg[pl.ds(2 * chip, 2)].reshape(64, 2048)
+        q_all[y, chip] = project(rows, wq)
+        send_q(y, i, y_right)
+        send_q(y, i, y_left)
+
+    def relay_q(i):
+        if i % 2 == 0:
+            got_q(yl, i)
+            send_q(yl, i, y_right)
+        else:
+            got_q(yr, i)
+            send_q(yr, i, y_left)
 
     from_left, from_right, from_far = 2 * xl + core, 2 * xr + core, 2 * x2 + core
 
@@ -241,6 +282,8 @@
     weights[1].wait()
     got_chip(x)
     project_kv(0)
+    weights[2].wait()
+    project_q(0)
     got_x(from_left, 0)
     send_x(xg.at[from_left, 0], from_left, 0, x_right)
     got_x(from_right, 1)
@@ -251,45 +294,23 @@
     send_x(xg.at[from_left, 1], from_left, 1, partner)
     got_x(from_right, 0)
     send_x(xg.at[from_right, 0], from_right, 0, partner)
+    pass_on(1, 0)
     got_chip(xl)
     project_kv(1)
     got_x(from_far, 0)
     send_x(xg.at[from_far, 0], from_far, 0, partner)
     got_x(from_far, 1)
     send_x(xg.at[from_far, 1], from_far, 1, partner)
+    project_q(1)
     got_chip(xr)
     project_kv(2)
     got_chip(x2)
     project_kv(3)
-
-    q_sent = []
-
-    def send_q(slot, half, device):
-        copy = remote(
-            q_all.at[slot, half],
-            q_all.at[slot, half],
-            q_send.at[len(q_sent)],
-            q_recv.at[slot, half],
-            device,
-        )
-        copy.start()
-        q_sent.append(copy)
-
-    def got_q(slot, half):
-        remote(
-            q_all.at[slot, half],
-            q_all.at[slot, half],
-            q_send.at[0],
-            q_recv.at[slot, half],
-            y_right,
-        ).wait_recv()
-    weights[2].wait()
+    project_q(2)
+    project_q(3)
+    pass_on(1, 1)
+
     whole_rows = xg[...].reshape(256, 2048)
-    q_all[y] = project(whole_rows, wq).reshape(2, 128, 256)
-    send_q(y, 0, y_right)
-    send_q(y, 1, y_left)
-    send_q(y, 1, y_right)
-    send_q(y, 0, y_left)
     weights[3].wait()
     pin[...] = project(whole_rows, wp)
     halo = remote(pin.at[pl.ds(240, 16)], rim, h_sem.at[0], h_sem.at[1], next_sp)
@@ -312,92 +333,107 @@
             shrink = jnp.exp2(before - peak)
             p = jnp.exp2(s - jnp.concatenate([peak, peak], axis=1))
             m_s[j, c] = peak
-            l_s[j, c] = l_s[j, c] * shrink + jnp.sum(p, axis=1, keepdims=True)
+            l_s[j, c] = l_s[j, c] * shrink + (p[:, :128] + p[:, 128:])
             pv = jnp.dot(p.astype(BF16), v, preferred_element_type=F32)
             acc[j, c] = acc[j, c] * jnp.concatenate([shrink, shrink], axis=1) + pv
 
-    def work(u):
-        first = u < Y
-        s = (u - Y) // 8 + 1
-        k = jnp.where(first, u, (u - Y) % 8)
-        up = k < Y
-        near = k % Y
-        j = (y + jnp.where(near == 3, 0, jnp.where(near == 2, 3, 2 - near))) % Y
-        slot = jnp.where(first, z, jnp.where(up, jnp.maximum(z - s, 0), (z + s) % zn))
+    partners = (y2, yr, yl, y)
+
+    def work(u, group):
+        s = u // 2 + 1
+        up = u % 2 == 0
+        slot = jnp.where(up, jnp.maximum(z - s, 0), (z + s) % zn)
         below = jnp.logical_and(up, s <= z)
         above = jnp.logical_and(z + s >= zn, jnp.logical_and(s < hops, jnp.logical_not(up)))
-        wanted = jnp.where(first, j > y, jnp.logical_or(below, above))
-
-        @pl.when(wanted)
-        def _():
-            attend(j, slot, False)
-
-    def work_until(done, ready, most):
-        count = jnp.minimum(ready - done, most)
-
-        def one(i, carry):
-            work(done + i)
-            return carry
-
-        lax.fori_loop(0, count, one, 0)
-        return done + count
-
-    pass_on(1, 0)
-    pass_on(1, 1)
+
+        @pl.when(jnp.logical_or(below, above))
+        def _():
+            for j in group:
+                attend(j, slot, False)
+
+    def work_once(done, ready):
+        @pl.when(done < ready)
+        def _():
+            work(done, partners)
+
+        return jnp.minimum(done + 1, ready)
+
+    def pooling():
+        halo.wait()
+        ext[pl.ds(0, 16), :] = jnp.where(sp > 0, rim[...].astype(F32), 0.0)
+        ext[pl.ds(16, 256), :] = pin[...].astype(F32)
+        width = jnp.left_shift(jnp.int32(2), tp % 4)
+        window = jnp.zeros((256, 128), F32)
+        for offset in range(16):
+            window = window + jnp.where(offset < width, ext[pl.ds(16 - offset, 256), :], 0.0)
+        position = sp * 256 + lax.broadcasted_iota(jnp.int32, (256, 128), 0)
+        counts = jnp.minimum(position + 1, width).astype(F32)
+        spread = (window / counts - ext[pl.ds(16, 256), :]).astype(BF16)
+        weights[6].wait()
+        pool_out = jnp.dot(spread, pool_weight[0], preferred_element_type=F32).astype(BF16)
+        weights[4].wait()
+        for n in range(8):
+            cols = slice(256 * n, 256 * n + 256)
+            pool_part[:, cols] = jnp.dot(pool_out, pow_[:, cols], preferred_element_type=F32)
+        for copy in weights[5:]:
+            if copy is not weights[6]:
+                copy.wait()
+    pass_on(2, 0)
+    relay_q(0)
+    relay_q(1)
     attend(y, z, True)
     pass_on(1, 2)
-    halo.wait()
-    ext[pl.ds(0, 16), :] = jnp.where(sp > 0, rim[...].astype(F32), 0.0)
-    ext[pl.ds(16, 256), :] = pin[...].astype(F32)
-    width = jnp.left_shift(jnp.int32(2), tp % 4)
-    window = jnp.zeros((256, 128), F32)
-    for offset in range(16):
-        window = window + jnp.where(offset < width, ext[pl.ds(16 - offset, 256), :], 0.0)
-    position = sp * 256 + lax.broadcasted_iota(jnp.int32, (256, 128), 0)
-    counts = jnp.minimum(position + 1, width).astype(F32)
-    spread = (window / counts - ext[pl.ds(16, 256), :]).astype(BF16)
-    weights[6].wait()
-    pool_out = jnp.dot(spread, pool_weight[0], preferred_element_type=F32).astype(BF16)
-    weights[4].wait()
-    for n in range(8):
-        cols = slice(256 * n, 256 * n + 256)
-        pool_part[:, cols] = jnp.dot(pool_out, pow_[:, cols], preferred_element_type=F32)
-    for copy in weights[5:]:
-        if copy is not weights[6]:
-            copy.wait()
+    relay_q(2)
+    relay_q(3)
     pass_on(1, 3)
-    got_q(yl, 0)
-    send_q(yl, 0, y_right)
-    got_q(yr, 1)
-    send_q(yr, 1, y_left)
-    pass_on(2, 0)
-    got_q(yl, 1)
-    got_q(yr, 0)
-    pass_on(2, 1)
-    got_q(y2, 0)
-    got_q(y2, 1)
-    done = work_until(0, 4 + 8, 3)
-    pass_on(2, 2)
-    done = work_until(done, 4 + 8, 3)
-    pass_on(2, 3)
-    done = work_until(done, 4 + 16, 3)
+    for i in range(4):
+        if i % 2 == 0:
+            got_q(yr, i)
+        else:
+            got_q(yl, i)
+    for i in range(4):
+        got_q(y2, i)
+    def own_step(j, carry):
+        @pl.when(j > y)
+        def _():
+            attend(j, z, False)
+
+        return carry
+
+    lax.fori_loop(0, Y, own_step, 0)
 
     def ring_step(s, done):
-        for i in range(4):
-            pass_on(s, i)
-            done = work_until(done, Y + 8 * (s if i == 3 else s - 1), 3)
+        pass_on(s, 1)
+        done = work_once(done, 2 * (s - 1))
+        pass_on(s + 1, 0)
+        done = work_once(done, 2 * (s - 1))
+        pass_on(s, 2)
+        done = work_once(done, 2 * (s - 1))
+
+        @pl.when(s == hops // 2 + 1)
+        def _():
+            pooling()
+        pass_on(s, 3)
         return done
 
-    done = lax.fori_loop(3, hops, ring_step, done)
-    pass_on(hops, 0)
+    done = lax.fori_loop(2, hops, ring_step, 0)
     pass_on(hops, 2)
-    done = work_until(done, Y + 8 * (hops - 1), 3)
+    done = work_once(done, 2 * (hops - 1))
     pass_on(hops, 1)
+    done = lax.fori_loop(
+        done, 2 * (hops - 1), lambda i, d: work_once(d, 2 * (hops - 1)), done
+    )
     pass_on(hops, 3)
-    work_until(done, Y + 8 * (hops - 1), 99)
     def state(j, half):
         rows = pl.ds(128 * half, 128)
-        return [(m_s[j, c, rows, :], l_s[j, c, rows, :], acc[j, c, rows, :]) for c in range(2)]
+        return [
+            (
+                m_s[j, c, rows, :],
+                jnp.broadcast_to(jnp.sum(l_s[j, c, rows, :], axis=1, keepdims=True), (128, 128)),
+                acc[j, c, rows, :],
+            )
+            for c in range(2)
+        ]
 
     def arrived(payload, stats):
         columns = jnp.concatenate([stats[...], jnp.zeros((120, 128), F32)], axis=0).T
@@ -440,15 +476,13 @@
                 src.at[index], dst, ps_send.at[index, i], ps_recv.at[index, i], y_right
             ).wait_recv()
 
-    base = Y + 8 * (hops - 1)
-    work(base)
+    base = 2 * (hops - 1)
+    work(base, (y2, yr))
     send_state(state(y2, 0), 0, r2.at[0], r2t.at[0], y_right)
     send_state(state(y2, 1), 1, r2.at[1], r2t.at[1], y_left)
-    work(base + 1)
     send_state(state(yr, 1), 2, rn.at[0, 1], rnt.at[0, 1], y_right)
-    work(base + 2)
+    work(base, (yl, y))
     send_state(state(yl, 0), 3, rn.at[1, 0], rnt.at[1, 0], y_left)
-    work(base + 3)
     got_state(0, r2.at[0], r2t.at[0])
     send_state(
         joined(state(yr, 0), arrived(r2.at[0], r2t.at[0])), 4, rn.at[0, 0], rnt.at[0, 0], y_right
@@ -480,14 +514,9 @@
         cols = slice(256 * n, 256 * n + 256)
         tile = jnp.dot(mixed, cow[:, cols], preferred_element_type=F32) + pool_part[:, cols]
         part[:, :, :, :, cols] = tile.astype(BF16).reshape(X, 2, 2, 16, 256)
-    pair = [
-        remote(part.at[xx, 1 - core], pr.at[xx], pr_send.at[xx], pr_recv.at[xx], partner)
-        for xx in range(X)
-    ]
-    for copy in pair:
-        copy.start()
-    for copy in pair:
-        copy.wait_recv()
+    pair = remote(part.at[:, 1 - core], pr, pr_send.at[0], pr_recv.at[0], partner)
+    pair.start()
+    pair.wait_recv()
     def both(owner, half):
         return part[owner, core, half].astype(F32) + pr[owner, half].astype(F32)
 
@@ -517,24 +546,11 @@
     for half in range(2):
         total = both(x, half) + xrn[0, half].astype(F32) + xrn[1, half].astype(F32)
         out[pl.ds(16 * half, 16), :] = total.astype(BF16)
-    for copy in sent + q_sent + y_sent + pair + x_sent:
+    for copy in sent + q_sent + y_sent + [pair] + x_sent:
         copy.wait_send()
 
-    def drain(s, carry):
-        for i in range(4):
-            up, dn = sends(s, i)
-
-            @pl.when(up)
-            def _():
-                kv_copy(jnp.maximum(z - s, 0), i, s, True).wait_send()
-
-            @pl.when(dn)
-            def _():
-                kv_copy((z + s) % zn, i, s, False).wait_send()
-
-        return carry
-
-    lax.fori_loop(0, hops, drain, 0)
+    for i in range(4):
+        kv_left(hops - 1, i)
 
 
 def solution(mesh):
@@ -571,7 +587,7 @@
                 V((1, 128, 128), BF16),
                 V((1, 256), F32),
                 pltpu.SMEM((8,), F32),
-                V((Y, 2, 128, 256), BF16),
+                V((Y, X, 64, 256), BF16),
                 V((zn, X, 64, 512), BF16),
                 V((Y, 2, 256, 256), F32),
                 V((Y, 2, 256, 128), F32),
@@ -595,17 +611,16 @@
                 dma((11,)),
                 dma((14,)),
                 dma((8, 2)),
-                dma((zn // 2, X)),
-                dma((zn // 2, X)),
+                dma((2, X)),
+                dma((2, X)),
                 dma((zn, X)),
-                dma((zn, X)),
-                dma((6,)),
-                dma((Y, 2)),
+                dma((12,)),
+                dma((Y, X)),
                 dma((2,)),
                 dma((6, 2)),
                 dma((6, 2)),
-                dma((X,)),
-                dma((X,)),
+                dma((1,)),
+                dma((1,)),
                 dma((6,)),
                 dma((6,)),
             ],

time: 84.2 us -> 82.7 us (0.982)
  the two profiles are of different devices: /device:TPU:451 before, /device:TPU:1 now
where the time goes in v3:
time: 82.7 us; the launch traced here: 82.6 us
  Pallas kernels  81 us (98%)
  local copies, waits for them, and re-layouts  1.57 us (2%)
    pallas_call x1, Pallas kernels, per_device(): pl.pallas_call(functools.partial(kernel, zn), out_shape=jax.ShapeDtypeStr...  81 us

profile of v3, /device:TPU:1, one launch (start us, length us, event | category | flops | bytes accessed | tf_op | source)
XLA Modules:
  0.0 82.6 jit_solution(17425133213660153434)
XLA Ops:
  0.0 81.0 %shard_map.100 = bf16[32,2048]{1,0:T(8,128)(2,1)} custom-call(bf16[32,2048]{1,0:T(8,128)(2,1)} %normed_h.1, bf16[2048,256]{1,0:T(8,128)(2,1)} %wq_h.1, bf16[2048,256]{1,0:T(8,128)(2,1)} %wk_h.1, bf16[2048,256]{1,0:T(8,128)(2,1)} %wv_h.1, bf16[2048,128]{1,0:T(8,128)(2,1)} %wp_h.1, bf16[1,128,128]{2,1,0:T(8,128)(2,1)} %pool_weight_h.1, f32[8]{0:T(128)} %balance_h.1, ...), custom_call_target="tpu_custom_call" | custom-call | tf_op jit(solution)/shard_map/pallas_call | solution.py:575
  81.0 1.6 %copy.12 = bf16[32,2048]{1,0:T(8,128)(2,1)} copy(bf16[32,2048]{1,0:T(8,128)(2,1)} %shard_map.100) | data formatting | bytes 262144

commit v4 on v3

--- a/solution.py
+++ b/solution.py
@@ -290,11 +290,11 @@
     send_x(xg.at[from_right, 1], from_right, 1, x_left)
     send_x(xg.at[from_left, 0], from_left, 0, partner)
     send_x(xg.at[from_right, 1], from_right, 1, partner)
+    pass_on(1, 0)
     got_x(from_left, 1)
     send_x(xg.at[from_left, 1], from_left, 1, partner)
     got_x(from_right, 0)
     send_x(xg.at[from_right, 0], from_right, 0, partner)
-    pass_on(1, 0)
     got_chip(xl)
     project_kv(1)
     got_x(from_far, 0)
@@ -304,6 +304,7 @@
     project_q(1)
     got_chip(xr)
     project_kv(2)
+    pass_on(2, 0)
     got_chip(x2)
     project_kv(3)
     project_q(2)
@@ -378,13 +379,13 @@
         for copy in weights[5:]:
             if copy is not weights[6]:
                 copy.wait()
-    pass_on(2, 0)
     relay_q(0)
     relay_q(1)
     attend(y, z, True)
     pass_on(1, 2)
     relay_q(2)
     relay_q(3)
+    pass_on(3, 0)
     pass_on(1, 3)
     for i in range(4):
         if i % 2 == 0:
@@ -405,7 +406,7 @@
     def ring_step(s, done):
         pass_on(s, 1)
         done = work_once(done, 2 * (s - 1))
-        pass_on(s + 1, 0)
+        pass_on(s + 2, 0)
         done = work_once(done, 2 * (s - 1))
         pass_on(s, 2)
         done = work_once(done, 2 * (s - 1))
@@ -417,6 +418,7 @@
         return done
 
     done = lax.fori_loop(2, hops, ring_step, 0)
+    done = work_once(done, 2 * (hops - 1))
     pass_on(hops, 2)
     done = work_once(done, 2 * (hops - 1))
     pass_on(hops, 1)
@@ -549,7 +551,7 @@
     for copy in sent + q_sent + y_sent + [pair] + x_sent:
         copy.wait_send()
 
-    for i in range(4):
+    for i in range(1, 4):
         kv_left(hops - 1, i)
 
 
@@ -574,7 +576,7 @@
         V = pltpu.VMEM
         return pl.pallas_call(
             functools.partial(kernel, zn),
-            out_shape=jax.ShapeDtypeStruct(normed.shape, BF16),
+            out_shape=pltpu.VMEM(normed.shape, BF16),
             in_specs=[hbm] * 10,
             out_specs=vmem,
             scratch_shapes=[
@@ -625,7 +627,7 @@
                 dma((6,)),
             ],
             compiler_params=pltpu.CompilerParams(
-                collective_id=0, has_side_effects=True, vmem_limit_bytes=67043328
+                collective_id=0, has_side_effects=True, vmem_limit_bytes=66900000
             ),
         )(
             normed,

time: 82.7 us -> 80.6 us (0.975)
  Pallas kernels: 81 us -> 79.8 us
  local copies, waits for them, and re-layouts: 1.57 us -> 0.66 us
    pallas_call x1, Pallas kernels: 81 us -> 79.8 us  [per_device(): pl.pallas_call(functools.partial(kernel, zn), out_shape=pltpu.VMEM(normed...]
    unnamed x1, local copies, waits for them, and re-layouts: 1.57 us -> 0.66 us
where the time goes in v4:
time: 80.6 us; the launch traced here: 80.5 us
  Pallas kernels  79.8 us (99%)
    pallas_call x1, Pallas kernels, per_device(): pl.pallas_call(functools.partial(kernel, zn), out_shape=pltpu.VMEM(normed...  79.8 us

profile of v4, /device:TPU:1, one launch (start us, length us, event | category | flops | bytes accessed | tf_op | source)
XLA Modules:
  0.0 80.5 jit_solution(15070956248531321055)
XLA Ops:
  0.0 79.8 %shard_map.100 = bf16[32,2048]{1,0:T(8,128)(2,1)S(1)} custom-call(bf16[32,2048]{1,0:T(8,128)(2,1)} %normed_h.1, bf16[2048,256]{1,0:T(8,128)(2,1)} %wq_h.1, bf16[2048,256]{1,0:T(8,128)(2,1)} %wk_h.1, bf16[2048,256]{1,0:T(8,128)(2,1)} %wv_h.1, bf16[2048,128]{1,0:T(8,128)(2,1)} %wp_h.1, bf16[1,128,128]{2,1,0:T(8,128)(2,1)} %pool_weight_h.1, f32[8]{0:T(128)} %balance_h.1, ...), custom_call_target="tpu_custom_call" | custom-call | tf_op jit(solution)/shard_map/pallas_call | solution.py:577
  79.8 0.7 copy.12

commit v5 on v4

--- a/solution.py
+++ b/solution.py
@@ -69,11 +69,8 @@
     q_send,
     q_recv,
     h_sem,
-    ps_send,
     ps_recv,
-    pr_send,
     pr_recv,
-    xs_send,
     xs_recv,
 ):
     sp = lax.axis_index("sp")
@@ -184,14 +181,13 @@
         dn = jnp.logical_and(dn, s + 1 <= (hops if i >= 2 else hops - 1))
         return up, dn
 
-    def kv_left(s, i):
-        up, dn = sends(s, i)
-
-        @pl.when(up)
+    def left_up(s, i):
+        @pl.when(sends(s, i)[0])
         def _():
             kv_copy(jnp.maximum(z - s, 0), i, s, True).wait_send()
 
-        @pl.when(dn)
+    def left_down(s, i):
+        @pl.when(sends(s, i)[1])
         def _():
             kv_copy((z + s) % zn, i, s, False).wait_send()
 
@@ -206,29 +202,36 @@
         def _():
             kv_copy((z + s) % zn, i, s, False).start()
 
+    def pass_up(s, i):
+        here = jnp.logical_and(s <= z, s <= (hops if i < 2 else hops - 1))
+        if not (isinstance(s, int) and s < 2):
+            left_up(s - 2, i)
+
+        @pl.when(here)
+        def _():
+            kv_copy(jnp.maximum(z - s, 0), i, 0, True).wait_recv()
+
+        @pl.when(sends(s, i)[0])
+        def _():
+            kv_copy(jnp.maximum(z - s, 0), i, s, True).start()
+
+    def pass_down(s, i):
+        here = (z + s) % zn <= (hops - 1 if i >= 2 else hops - 2)
+        here = jnp.logical_and(here, s <= (hops if i >= 2 else hops - 1))
+        if not (isinstance(s, int) and s < 2):
+            left_down(s - 2, i)
+
+        @pl.when(here)
+        def _():
+            kv_copy((z + s) % zn, i, 0, False).wait_recv()
+
+        @pl.when(sends(s, i)[1])
+        def _():
+            kv_copy((z + s) % zn, i, s, False).start()
+
     def pass_on(s, i):
-        up_here = jnp.logical_and(s <= z, s <= (hops if i < 2 else hops - 1))
-        dn_here = (z + s) % zn <= (hops - 1 if i >= 2 else hops - 2)
-        dn_here = jnp.logical_and(dn_here, s <= (hops if i >= 2 else hops - 1))
-        up, dn = sends(s, i)
-        if not (isinstance(s, int) and s < 2):
-            kv_left(s - 2, i)
-
-        @pl.when(up_here)
-        def _():
-            kv_copy(jnp.maximum(z - s, 0), i, 0, True).wait_recv()
-
-        @pl.when(up)
-        def _():
-            kv_copy(jnp.maximum(z - s, 0), i, s, True).start()
-
-        @pl.when(dn_here)
-        def _():
-            kv_copy((z + s) % zn, i, 0, False).wait_recv()
-
-        @pl.when(dn)
-        def _():
-            kv_copy((z + s) % zn, i, s, False).start()
+        pass_up(s, i)
+        pass_down(s, i)
 
     def project(rows, weight):
         return jnp.dot(rows, weight[...], preferred_element_type=F32).astype(BF16)
@@ -394,6 +397,8 @@
             got_q(yl, i)
     for i in range(4):
         got_q(y2, i)
+    pass_down(2, 1)
+
     def own_step(j, carry):
         @pl.when(j > y)
         def _():
@@ -401,31 +406,39 @@
 
         return carry
 
-    lax.fori_loop(0, Y, own_step, 0)
-
     def ring_step(s, done):
-        pass_on(s, 1)
-        done = work_once(done, 2 * (s - 1))
+        pass_up(s, 1)
+        pass_down(s, 2)
+        @pl.when(s == 2)
+        def _():
+            lax.fori_loop(0, Y, own_step, 0)
+
+        done = work_once(done, jnp.where(s == 2, 0, 2 * (s - 1)))
         pass_on(s + 2, 0)
         done = work_once(done, 2 * (s - 1))
-        pass_on(s, 2)
+        pass_up(s, 2)
+        pass_down(s, 3)
         done = work_once(done, 2 * (s - 1))
 
         @pl.when(s == hops // 2 + 1)
         def _():
             pooling()
-        pass_on(s, 3)
+        pass_up(s, 3)
+        pass_down(s + 1, 1)
         return done
 
     done = lax.fori_loop(2, hops, ring_step, 0)
+    for copy in sent + q_sent:
+        copy.wait_send()
     done = work_once(done, 2 * (hops - 1))
-    pass_on(hops, 2)
+    pass_down(hops, 2)
     done = work_once(done, 2 * (hops - 1))
-    pass_on(hops, 1)
+    for i in (1, 2, 3):
+        pass_up(hops, i)
     done = lax.fori_loop(
         done, 2 * (hops - 1), lambda i, d: work_once(d, 2 * (hops - 1)), done
     )
-    pass_on(hops, 3)
+    pass_down(hops, 3)
     def state(j, half):
         rows = pl.ds(128 * half, 128)
         return [
@@ -468,22 +481,22 @@
         ps[index, :, :256] = a0.astype(BF16)
         ps[index, :, 256:] = a1.astype(BF16)
         for i, (src, dst) in enumerate(((ps, payload), (pst, stats))):
-            copy = remote(src.at[index], dst, ps_send.at[index, i], ps_recv.at[index, i], device)
+            copy = remote(src.at[index], dst, q_send.at[2 * index + i], ps_recv.at[index, i], device)
             copy.start()
             y_sent.append(copy)
 
     def got_state(index, payload, stats):
         for i, (src, dst) in enumerate(((ps, payload), (pst, stats))):
             remote(
-                src.at[index], dst, ps_send.at[index, i], ps_recv.at[index, i], y_right
+                src.at[index], dst, q_send.at[2 * index + i], ps_recv.at[index, i], y_right
             ).wait_recv()
 
     base = 2 * (hops - 1)
-    work(base, (y2, yr))
+    work(base, (y2,))
     send_state(state(y2, 0), 0, r2.at[0], r2t.at[0], y_right)
     send_state(state(y2, 1), 1, r2.at[1], r2t.at[1], y_left)
+    work(base, (yr, yl, y))
     send_state(state(yr, 1), 2, rn.at[0, 1], rnt.at[0, 1], y_right)
-    work(base, (yl, y))
     send_state(state(yl, 0), 3, rn.at[1, 0], rnt.at[1, 0], y_left)
     got_state(0, r2.at[0], r2t.at[0])
     send_state(
@@ -516,9 +529,15 @@
         cols = slice(256 * n, 256 * n + 256)
         tile = jnp.dot(mixed, cow[:, cols], preferred_element_type=F32) + pool_part[:, cols]
         part[:, :, :, :, cols] = tile.astype(BF16).reshape(X, 2, 2, 16, 256)
-    pair = remote(part.at[:, 1 - core], pr, pr_send.at[0], pr_recv.at[0], partner)
-    pair.start()
-    pair.wait_recv()
+    pair = [
+        remote(
+            part.at[chip, 1 - core], pr.at[chip], xg_send.at[6 + i], pr_recv.at[i], partner
+        )
+        for i, chip in enumerate((x2, xr, xl, x))
+    ]
+    for copy in pair:
+        copy.start()
+    pair[0].wait_recv()
     def both(owner, half):
         return part[owner, core, half].astype(F32) + pr[owner, half].astype(F32)
 
@@ -526,21 +545,24 @@
 
     def send_sum(value, index, dst, device):
         xs[index] = value.astype(BF16)
-        copy = remote(xs.at[index], dst, xs_send.at[index], xs_recv.at[index], device)
+        copy = remote(xs.at[index], dst, xg_send.at[index], xs_recv.at[index], device)
         copy.start()
         x_sent.append(copy)
 
     def got_sum(index, dst):
-        remote(xs.at[index], dst, xs_send.at[index], xs_recv.at[index], x_right).wait_recv()
+        remote(xs.at[index], dst, xg_send.at[index], xs_recv.at[index], x_right).wait_recv()
 
     send_sum(both(x2, 0), 0, xr2.at[0], x_right)
     send_sum(both(x2, 1), 1, xr2.at[1], x_left)
+    pair[1].wait_recv()
+    pair[2].wait_recv()
     send_sum(both(xr, 1), 2, xrn.at[0, 1], x_right)
     send_sum(both(xl, 0), 3, xrn.at[1, 0], x_left)
     got_sum(0, xr2.at[0])
     send_sum(both(xr, 0) + xr2[0].astype(F32), 4, xrn.at[0, 0], x_right)
     got_sum(1, xr2.at[1])
     send_sum(both(xl, 1) + xr2[1].astype(F32), 5, xrn.at[1, 1], x_left)
+    pair[3].wait_recv()
     got_sum(2, xrn.at[0, 1])
     got_sum(3, xrn.at[1, 0])
     got_sum(4, xrn.at[0, 0])
@@ -548,11 +570,12 @@
     for half in range(2):
         total = both(x, half) + xrn[0, half].astype(F32) + xrn[1, half].astype(F32)
         out[pl.ds(16 * half, 16), :] = total.astype(BF16)
-    for copy in sent + q_sent + y_sent + [pair] + x_sent:
+    for copy in y_sent + pair + x_sent:
         copy.wait_send()
 
     for i in range(1, 4):
-        kv_left(hops - 1, i)
+        left_up(hops - 1, i)
+        left_down(hops - 1, i)
 
 
 def solution(mesh):
@@ -620,10 +643,7 @@
                 dma((Y, X)),
                 dma((2,)),
                 dma((6, 2)),
-                dma((6, 2)),
-                dma((1,)),
-                dma((1,)),
-                dma((6,)),
+                dma((X,)),
                 dma((6,)),
             ],
             compiler_params=pltpu.CompilerParams(

time: 80.6 us -> 80.4 us (level)
  no operation moved by 1% of the time
where the time goes in v5:
time: 80.4 us; the launch traced here: 80.3 us
  Pallas kernels  79.6 us (99%)
    pallas_call x1, Pallas kernels, per_device(): pl.pallas_call(functools.partial(kernel, zn), out_shape=pltpu.VMEM(normed...  79.6 us

profile of v5, /device:TPU:1, one launch (start us, length us, event | category | flops | bytes accessed | tf_op | source)
XLA Modules:
  0.0 80.3 jit_solution(7498942746156971799)
XLA Ops:
  0.0 79.6 %shard_map.100 = bf16[32,2048]{1,0:T(8,128)(2,1)S(1)} custom-call(bf16[32,2048]{1,0:T(8,128)(2,1)} %normed_h.1, bf16[2048,256]{1,0:T(8,128)(2,1)} %wq_h.1, bf16[2048,256]{1,0:T(8,128)(2,1)} %wk_h.1, bf16[2048,256]{1,0:T(8,128)(2,1)} %wv_h.1, bf16[2048,128]{1,0:T(8,128)(2,1)} %wp_h.1, bf16[1,128,128]{2,1,0:T(8,128)(2,1)} %pool_weight_h.1, f32[8]{0:T(128)} %balance_h.1, ...), custom_call_target="tpu_custom_call" | custom-call | tf_op jit(solution)/shard_map/pallas_call | solution.py:600
  79.6 0.7 copy.12

commit v6 on v5

--- a/solution.py
+++ b/solution.py
@@ -123,6 +123,11 @@
     peers = (partner, x_right, x_left, y_right, y_left, z_up, z_down, next_sp, prev_sp)
     for peer in peers:
         pl.semaphore_signal(barrier, inc=1, device_id=peer, device_id_type=MESH)
+    for j in range(Y):
+        for c in range(2):
+            m_s[j, c] = jnp.full((256, 128), NEG, F32)
+            l_s[j, c] = jnp.zeros((256, 128), F32)
+            acc[j, c] = jnp.zeros((256, 256), F32)
     pl.semaphore_wait(barrier, len(peers))
     for copy in rows_in:
         copy.wait()
@@ -276,11 +281,6 @@
     def got_chip(chip):
         for half in range(2):
             got_x(2 * chip + 1 - core, half)
-    for j in range(Y):
-        for c in range(2):
-            m_s[j, c] = jnp.full((256, 128), NEG, F32)
-            l_s[j, c] = jnp.zeros((256, 128), F32)
-            acc[j, c] = jnp.zeros((256, 256), F32)
     weights[0].wait()
     weights[1].wait()
     got_chip(x)
@@ -398,6 +398,7 @@
     for i in range(4):
         got_q(y2, i)
     pass_down(2, 1)
+    pass_down(2, 2)
 
     def own_step(j, carry):
         @pl.when(j > y)
@@ -408,7 +409,7 @@
 
     def ring_step(s, done):
         pass_up(s, 1)
-        pass_down(s, 2)
+        pass_down(s, 3)
         @pl.when(s == 2)
         def _():
             lax.fori_loop(0, Y, own_step, 0)
@@ -417,21 +418,20 @@
         pass_on(s + 2, 0)
         done = work_once(done, 2 * (s - 1))
         pass_up(s, 2)
-        pass_down(s, 3)
+        pass_down(s + 1, 1)
         done = work_once(done, 2 * (s - 1))
 
         @pl.when(s == hops // 2 + 1)
         def _():
             pooling()
         pass_up(s, 3)
-        pass_down(s + 1, 1)
+        pass_down(s + 1, 2)
         return done
 
     done = lax.fori_loop(2, hops, ring_step, 0)
     for copy in sent + q_sent:
         copy.wait_send()
     done = work_once(done, 2 * (hops - 1))
-    pass_down(hops, 2)
     done = work_once(done, 2 * (hops - 1))
     for i in (1, 2, 3):
         pass_up(hops, i)

time: 80.4 us -> 80.4 us (level)
  no operation moved by 1% of the time
where the time goes in v6:
time: 80.4 us; the launch traced here: 80.3 us
  Pallas kernels  79.6 us (99%)
    pallas_call x1, Pallas kernels, per_device(): pl.pallas_call(functools.partial(kernel, zn), out_shape=pltpu.VMEM(normed...  79.6 us

profile of v6, /device:TPU:1, one launch (start us, length us, event | category | flops | bytes accessed | tf_op | source)
XLA Modules:
  0.0 80.3 jit_solution(8337610676364012833)
XLA Ops:
  0.0 79.6 %shard_map.100 = bf16[32,2048]{1,0:T(8,128)(2,1)S(1)} custom-call(bf16[32,2048]{1,0:T(8,128)(2,1)} %normed_h.1, bf16[2048,256]{1,0:T(8,128)(2,1)} %wq_h.1, bf16[2048,256]{1,0:T(8,128)(2,1)} %wk_h.1, bf16[2048,256]{1,0:T(8,128)(2,1)} %wv_h.1, bf16[2048,128]{1,0:T(8,128)(2,1)} %wp_h.1, bf16[1,128,128]{2,1,0:T(8,128)(2,1)} %pool_weight_h.1, f32[8]{0:T(128)} %balance_h.1, ...), custom_call_target="tpu_custom_call" | custom-call | tf_op jit(solution)/shard_map/pallas_call | solution.py:600
  79.6 0.7 copy.12
